TPU v7x, 256 devices: a 4x2x16 block of a 4x16x16 slice. The times are simulated.
256 devices in a mesh: grp: 2 (over y), ep: 32 (over z, core), tp: 4 (over x).
Axes of the slice: x: 4, y: 2, z: 16, core: 2. Of those that a mesh axis runs over, the one named last changes fastest.
The devices are a block of a 4x16x16 slice.
Arguments:
- queries: bfloat16 [16384, 1024], P(('grp', 'ep'), 'tp'), parts along dimension 0, may hold values from -6 to 6
- head_key_rows: bfloat16 [16384, 1024], P(('grp', 'ep'), 'tp'), parts along dimension 0, may hold values from -6 to 6
- head_value_rows: bfloat16 [16384, 2048], P(('grp', 'ep'), 'tp'), parts along dimension 0, may hold values from -6 to 6
- output_gate_logits: bfloat16 [16384, 2048], P(('grp', 'ep'), 'tp'), parts along dimension 0, may hold values from -6 to 6
- log_input_gate: float32 [4, 16384], P('tp', ('grp', 'ep')), parts along dimension 1, may hold values from -5 to 103
- forget_gate_logits: float32 [4, 16384], P('tp', ('grp', 'ep')), parts along dimension 1, may hold values from 1 to 20
- extra_log_forget: float32 [4, 16384], P('tp', ('grp', 'ep')), parts along dimension 1, may hold values from -1 to 0, as said below
- head_norm_gain: float32 [2048], P('tp'), may hold values from 0.1 to 1.9
- memory_output_matrix: bfloat16 [2048, 2048], P('tp'), may hold values from -0.125 to 0.125
- expert_input_tokens: bfloat16 [16384, 2048], P(('grp', 'ep', 'tp')), parts along dimension 0, may hold values from -6 to 6
- expert_norm_gain: float32 [2048], replicated, may hold values from 0.1 to 1.9
- routes: int32 [16384, 2], P(('grp', 'ep', 'tp')), parts along dimension 0, may hold values from 0 to 127, all different within a row; in each aligned block of 64 rows (0 to 63, 64 to 127, ...) at most 2 rows name the same one
- routed_expert_weight: float32 [16384, 2], P(('grp', 'ep', 'tp')), parts along dimension 0, may hold values from 0.1 to 1
- expert_gate_matrix: bfloat16 [128, 2048, 512], P(('ep', 'tp')), may hold values from -0.125 to 0.125
- expert_up_matrix: bfloat16 [128, 2048, 512], P(('ep', 'tp')), may hold values from -0.125 to 0.125
- expert_down_matrix: bfloat16 [128, 512, 2048], P(('ep', 'tp')), may hold values from -0.25 to 0.25
Outputs:
- mixer_out: bfloat16 [16384, 2048], P(('grp', 'ep', 'tp')), parts along dimension 0
- expert_out: bfloat16 [16384, 2048], P(('grp', 'ep', 'tp')), parts along dimension 0
There are 2 independent parts, one for each index of `grp`. A program takes and returns all parts, laid end to end along the dimension named above; an argument that names none is the same for every part. Nothing has to cross between parts.
Inputs may be any that keep to these rules, and one draw needn't show every extreme that they name: `routes`: each row names 2 different experts. In the rows of one device (aligned blocks of 64 rows) no expert is named more than 2 times, and in some blocks one expert is named exactly 2 times. `extra_log_forget`: mostly zero.
All inputs are finite; a program needn't handle non-finite values.
Results may differ from a plain program's by a relative error of at most 0.009.
Values may be sent and summed in bfloat16 or wider, within the bound.
A program may use at most 128 MiB of HBM per device.

v0:
```python
import jax
import jax.numpy as jnp
from jax import lax
from jax.sharding import Mesh
from jax.sharding import PartitionSpec as P

EP = ("ep_0", "ep_1")
EP_TP = ("ep_0", "ep_1", "tp")
GRP_EP = ("grp", "ep_0", "ep_1")
GRP_EP_TP = ("grp", "ep_0", "ep_1", "tp")


lowest_log = -1e30
norm_eps = 1e-06
layer_eps = 1e-05


def prefix(value, axis, join, neutral):
    count, mine = (lax.axis_size(axis), lax.axis_index(axis))
    pieces = jax.tree.map(lambda part: lax.all_gather(part, axis), value)
    so_far = jax.tree.map(
        lambda part, zero: jnp.full_like(part, 0) + jnp.asarray(zero, part.dtype), value, neutral
    )

    def lap(position, so_far):
        longer = join(so_far, jax.tree.map(lambda part: part[position], pieces))
        return jax.tree.map(lambda new, old: jnp.where(position < mine, new, old), longer, so_far)

    return lax.fori_loop(0, count - 1, lap, so_far)


def neutral_like(x, identity):
    return jax.tree.map(
        lambda part, zero: jnp.zeros_like(part) + jnp.asarray(zero, part.dtype), x, identity
    )


def carried_in(x, axes, combine, identity):
    before = start = neutral_like(x, identity)
    so_far = x
    for axis in reversed(axes):
        peers, mine = (lax.axis_size(axis), lax.axis_index(axis))
        pieces = jax.tree.map(lambda part: lax.all_gather(part, axis), so_far)
        inside, so_far = (start, start)
        for k in reversed(range(peers)):
            passed = k > mine
            so_far = combine(so_far, jax.tree.map(lambda part: part[k], pieces))
            inside = jax.tree.map(lambda new, old: jnp.where(passed, new, old), so_far, inside)
        before = combine(inside, before)
    return before


def in_blocks(x, dim, peers):
    dims = x.shape
    blocks = x.reshape(*dims[:dim], peers, dims[dim] // peers, *dims[dim + 1 :])
    return jnp.moveaxis(blocks, dim, 0)


def summed_on_arrival(x, axis, dim):
    blocks = in_blocks(x, dim, lax.axis_size(axis))
    arrived = lax.all_to_all(blocks, axis, split_axis=0, concat_axis=0, tiled=True)
    return arrived.astype(jnp.float32).sum(axis=0)


def join_states(earlier, later):
    early_memory, early_top, early_total = earlier
    late_memory, late_top, late_total = later
    joined_top = jnp.maximum(late_total + early_top, late_top)
    joined_memory = (
        jnp.exp(late_total + early_top - joined_top) * early_memory
        + jnp.exp(late_top - joined_top) * late_memory
    )
    return (joined_memory, joined_top, early_total + late_total)


def block_summary(keys_f32, values_f32, log_weight):
    top_weight = jnp.max(log_weight)
    weighted = keys_f32 * jnp.exp(log_weight - top_weight)[:, None]
    memory = jnp.einsum("sd,se->de", weighted, values_f32, precision=lax.Precision.HIGHEST)
    return (memory, top_weight)


def block_output(
    queries,
    head_key_rows,
    head_value_rows,
    output_gate_logits,
    in_gate,
    through,
    before,
    span_total,
    prior_memory,
    prior_top,
    later_memory,
    later_top,
    head_norm_gain,
):
    score_scale = queries.shape[1] ** (-0.5)
    from_prior = through + prior_top
    from_later = span_total - before + later_top
    fw_log = through[:, None] - through[None, :] + in_gate[None, :]
    bw_log = before[None, :] - before[:, None] + in_gate[None, :]
    positions = jnp.arange(queries.shape[0])
    lower_mask = positions[:, None] >= positions[None, :]
    upper_mask = positions[:, None] <= positions[None, :]
    inner_top = jnp.maximum(
        jnp.max(jnp.where(lower_mask, fw_log, -jnp.inf), axis=1),
        jnp.max(jnp.where(upper_mask, bw_log, -jnp.inf), axis=1),
    )
    row_top = jnp.maximum(inner_top, jnp.maximum(from_prior, from_later))
    weights = jnp.where(lower_mask, jnp.exp(fw_log - row_top[:, None]), 0.0) + jnp.where(
        upper_mask, jnp.exp(bw_log - row_top[:, None]), 0.0
    )
    scores = (
        jnp.einsum("td,sd->ts", queries, head_key_rows, preferred_element_type=jnp.float32)
        * score_scale
    )
    near_weights = (scores * weights).astype(jnp.bfloat16)
    queries_f32 = queries.astype(jnp.float32)
    carried = jnp.exp(from_prior - row_top)[:, None] * jnp.dot(
        queries_f32, prior_memory, precision=lax.Precision.HIGHEST
    )
    carried = carried + jnp.exp(from_later - row_top)[:, None] * jnp.dot(
        queries_f32, later_memory, precision=lax.Precision.HIGHEST
    )
    head_rows = (
        jnp.dot(near_weights, head_value_rows, preferred_element_type=jnp.float32)
        + carried * score_scale
    )
    normed = (
        head_rows
        * lax.rsqrt(jnp.mean(head_rows * head_rows, axis=1, keepdims=True) + norm_eps)
        * head_norm_gain
    )
    return (jax.nn.sigmoid(output_gate_logits.astype(jnp.float32)) * normed).astype(jnp.bfloat16)


def mixer_part(
    queries,
    head_key_rows,
    head_value_rows,
    output_gate_logits,
    log_input_gate,
    forget_gate_logits,
    extra_log_forget,
    head_norm_gain,
    memory_output_matrix,
):
    forget_log_value = jax.nn.log_sigmoid(forget_gate_logits[0]) + extra_log_forget[0]
    in_gate = log_input_gate[0]
    through = jnp.cumsum(forget_log_value)
    before = through - forget_log_value
    span_total = through[-1]
    keys_f32 = head_key_rows.astype(jnp.float32)
    values_f32 = head_value_rows.astype(jnp.float32)
    fw_memory, fw_top = block_summary(keys_f32, values_f32, span_total - through + in_gate)
    bw_memory, bw_top = block_summary(keys_f32, values_f32, before + in_gate)
    identity = (
        jnp.zeros_like(fw_memory),
        jnp.array(lowest_log, jnp.float32),
        jnp.array(0.0, jnp.float32),
    )
    prior_memory, prior_top, _ = prefix((fw_memory, fw_top, span_total), EP, join_states, identity)
    later_memory, later_top, _ = carried_in(
        (bw_memory, bw_top, span_total), EP, join_states, identity
    )
    gated_rows = block_output(
        queries,
        head_key_rows,
        head_value_rows,
        output_gate_logits,
        in_gate,
        through,
        before,
        span_total,
        prior_memory,
        prior_top,
        later_memory,
        later_top,
        head_norm_gain,
    )
    return summed_on_arrival(
        jnp.dot(gated_rows, memory_output_matrix, preferred_element_type=jnp.float32).astype(
            jnp.bfloat16
        ),
        "tp",
        0,
    ).astype(jnp.bfloat16)


def run_experts(arrived, expert_gate_matrix, expert_up_matrix, expert_down_matrix):
    gate_part = jnp.einsum(
        "nejd,edf->nejf", arrived, expert_gate_matrix, preferred_element_type=jnp.float32
    )
    up_part = jnp.einsum(
        "nejd,edf->nejf", arrived, expert_up_matrix, preferred_element_type=jnp.float32
    )
    hidden = (jax.nn.silu(gate_part) * up_part).astype(jnp.bfloat16)
    return jnp.einsum(
        "nejf,efd->nejd", hidden, expert_down_matrix, preferred_element_type=jnp.float32
    ).astype(jnp.bfloat16)


def expert_part(
    expert_input_tokens,
    expert_norm_gain,
    routes,
    routed_expert_weight,
    expert_gate_matrix,
    expert_up_matrix,
    expert_down_matrix,
):
    token_count, model_width = expert_input_tokens.shape
    top_count = routes.shape[1]
    local_experts = expert_gate_matrix.shape[0]
    ep_count = lax.axis_size(EP)
    tp_count = lax.axis_size("tp")
    devices = ep_count * tp_count
    expert_count = local_experts * devices
    capacity = max(2, 2 * token_count * top_count // expert_count)
    tokens_f32 = expert_input_tokens.astype(jnp.float32)
    centre = jnp.mean(tokens_f32, axis=1, keepdims=True)
    spread = jnp.mean(jnp.square(tokens_f32 - centre), axis=1, keepdims=True)
    normed = ((tokens_f32 - centre) * lax.rsqrt(spread + layer_eps) * expert_norm_gain).astype(
        jnp.bfloat16
    )
    flat_expert = routes.reshape(-1)
    one_hot = (flat_expert[:, None] == jnp.arange(expert_count, dtype=jnp.int32)[None, :]).astype(
        jnp.int32
    )
    earlier_count = jnp.cumsum(one_hot, axis=0) - one_hot
    slot_place = jnp.sum(earlier_count * one_hot, axis=1)
    slot_index = flat_expert * capacity + slot_place
    pair_row = jnp.arange(token_count * top_count, dtype=jnp.int32) // top_count
    source_row = jnp.zeros((expert_count * capacity,), jnp.int32).at[slot_index].set(pair_row)
    filled = jnp.zeros((expert_count * capacity,), jnp.int32).at[slot_index].set(1)
    outgoing = jnp.where(filled[:, None] > 0, normed[source_row], jnp.zeros((), jnp.bfloat16))
    results = run_experts(
        lax.all_to_all(
            outgoing.reshape(devices, local_experts, capacity, model_width),
            EP_TP,
            split_axis=0,
            concat_axis=0,
            tiled=True,
        ),
        expert_gate_matrix,
        expert_up_matrix,
        expert_down_matrix,
    )
    returned = lax.all_to_all(results, EP_TP, split_axis=0, concat_axis=0, tiled=True)
    returned = returned.reshape(expert_count * capacity, model_width)
    picked = returned[slot_index].reshape(token_count, top_count, model_width).astype(jnp.float32)
    combined = jnp.sum(routed_expert_weight[:, :, None] * picked, axis=1)
    return combined.astype(jnp.bfloat16)


def body(
    queries,
    head_key_rows,
    head_value_rows,
    output_gate_logits,
    log_input_gate,
    forget_gate_logits,
    extra_log_forget,
    head_norm_gain,
    memory_output_matrix,
    expert_input_tokens,
    expert_norm_gain,
    routes,
    routed_expert_weight,
    expert_gate_matrix,
    expert_up_matrix,
    expert_down_matrix,
):
    mixer_out = mixer_part(
        queries,
        head_key_rows,
        head_value_rows,
        output_gate_logits,
        log_input_gate,
        forget_gate_logits,
        extra_log_forget,
        head_norm_gain,
        memory_output_matrix,
    )
    expert_out = expert_part(
        expert_input_tokens,
        expert_norm_gain,
        routes,
        routed_expert_weight,
        expert_gate_matrix,
        expert_up_matrix,
        expert_down_matrix,
    )
    return (mixer_out, expert_out)


def solution(mesh):
    split = Mesh(
        mesh.devices.reshape(mesh.shape["grp"], 16, 2, mesh.shape["tp"]),
        ("grp", "ep_0", "ep_1", "tp"),
    )
    return jax.shard_map(
        body,
        mesh=split,
        in_specs=(
            P(GRP_EP, "tp"),
            P(GRP_EP, "tp"),
            P(GRP_EP, "tp"),
            P(GRP_EP, "tp"),
            P("tp", GRP_EP),
            P("tp", GRP_EP),
            P("tp", GRP_EP),
            P("tp"),
            P("tp", None),
            P(GRP_EP_TP, None),
            P(),
            P(GRP_EP_TP, None),
            P(GRP_EP_TP, None),
            P(EP_TP, None, None),
            P(EP_TP, None, None),
            P(EP_TP, None, None),
        ),
        out_specs=(P(GRP_EP_TP, None), P(GRP_EP_TP, None)),
        check_vma=False,
    )
```

profile of v0, /device:TPU:33, one launch (start us, length us, event | category | flops | bytes accessed | tf_op | source)
XLA Modules:
  0.0 456.2 jit_solution(11350778117073134547)
XLA Ops:
  11.4 2.3 fusion.125
  16.4 2.0 slice_dynamic-update-slice_fusion
  18.4 2.0 fusion.224
  20.5 2.0 subtract_exponential_fusion.3
  22.4 2.3 fusion.124
  26.3 22.6 %all-reduce.8 = (f32[2]{0:T(128)S(1)}, f32[2]{0:T(128)S(1)}) all-reduce(f32[2]{0:T(128)S(1)} %get-tuple-element.181, f32[2]{0:T(128)S(1)} %dynamic-update-slice.4), channel_id=1, replica_groups=mesh['grp'=2,'ep_0'=16,'ep_1'=2,'tp'=4] {'ep_1'}, use_global_device_ids=true, to_apply=%add.2 | all-reduce | flops 4 | bytes 32
  54.3 2.1 fusion.71
  59.5 1.5 gather.9
  62.2 3.2 fusion.27
  65.4 11.0 %all-to-all-start.1 = ((bf16[128,1,2,2048]{3,2,1,0:T(2,128)(2,1)}), bf16[128,1,2,2048]{3,2,1,0:T(2,128)(2,1)}, u32[]{:S(2)}, u32[]{:S(2)}) async-start(bf16[128,1,2,2048]{3,2,1,0:T(2,128)(2,1)} %fusion.27), calls=%async_computation.1 | async-start | bytes 2097152 | tf_op jit(solution)/shard_map/all_to_all | solution.py:239
  79.9 75.9 %all-reduce.7 = (f32[16]{0:T(128)S(1)}, f32[16]{0:T(128)S(1)}) all-reduce(f32[16]{0:T(128)S(1)} %dynamic-update-slice.3, f32[16]{0:T(128)S(1)} %dynamic-update-slice.5), channel_id=1, replica_groups=mesh['grp'=2,'ep_0'=16,'ep_1'=2,'tp'=4] {'ep_0'}, use_global_device_ids=true, to_apply=%add.3 | all-reduce | flops 32 | bytes 256
  190.8 52.3 %all-reduce.6 = (f32[32]{0:T(128)S(1)}, f32[32]{0:T(128)S(1)}) all-reduce(f32[32]{0:T(128)S(1)} %get-tuple-element.182, f32[32]{0:T(128)S(1)} %dynamic-update-slice.1), channel_id=1, replica_groups=mesh['grp'=2,'ep_0'=16,'ep_1'=2,'tp'=4] {'ep_0','ep_1'}, use_global_device_ids=true, to_apply=%add | all-reduce | flops 64 | bytes 512
  243.4 2.7 fusion.7
  246.1 4.3 fusion.1
  250.4 3.3 copy.38
  253.7 16.0 %all-to-all-start.2 = ((bf16[128,1,2,2048]{3,2,1,0:T(2,128)(2,1)}), bf16[128,1,2,2048]{3,2,1,0:T(2,128)(2,1)}, u32[]{:S(2)}, u32[]{:S(2)}) async-start(bf16[128,1,2,2048]{3,2,1,0:T(2,128)(2,1)} %copy.38), calls=%async_computation.2 | async-start | bytes 2097152 | tf_op jit(solution)/shard_map/all_to_all | solution.py:250
  269.8 147.3 %while.16 = (s32[]{:T(128)}, f32[256,512]{1,0:T(8,128)S(1)}, f32[]{:T(128)}, s32[]{:T(128)}, f32[32]{0:T(128)S(1)}, /*index=5*/f32[32]{0:T(128)S(1)}, f32[32,256,512]{2,1,0:T(8,128)}, s32[]{:T(128)}, s32[]{:T(128)}) while((s32[]{:T(128)}, f32[256,512]{1,0:T(8,128)S(1)}, f32[]{:T(128)}, s32[]{:T(128)}, f32[32]{0:T(128)S(1)}, ...), condition=%wide.region_6.7_spmd.clone, body=%wide.region_5.6_spmd.clone.sunk | while | flops 655369 | bytes 1573098 | solution.py:29
  273.1 1.5 fusion.241
  277.8 1.5 fusion.241
  282.6 1.5 fusion.241
  287.3 1.5 fusion.241
  292.1 1.5 fusion.241
  296.8 1.5 fusion.241
  301.6 1.5 fusion.241
  306.3 1.5 fusion.241
  311.1 1.5 fusion.241
  315.8 1.5 fusion.241
  320.6 1.5 fusion.241
  325.3 1.5 fusion.241
  330.1 1.5 fusion.241
  334.8 1.5 fusion.241
  339.6 1.5 fusion.241
  344.4 1.5 fusion.241
  349.1 1.5 fusion.241
  353.9 1.5 fusion.241
  358.6 1.5 fusion.241
  363.4 1.5 fusion.241
  368.1 1.5 fusion.241
  419.0 6.3 %fusion.18 = f32[256,512]{1,0:T(8,128)} fusion(f32[512,256]{0,1:T(8,128)} %convolution_multiply_fusion.1, bf16[256,256]{1,0:T(8,128)(2,1)S(1)} %copy-done.5, f32[16,256,512]{2,1,0:T(8,128)} %all-gather.6.cloned.1.call-done, f32[1,256,512]{2,1,0:T(8,128)S(1)} %copy-done.2, f32[512,512]{1,0:T(8,128)} %all-gather.10.cloned.1.call-done, f32[]{:T(128)S(6)} %exp.220, ...), kind=kOutput, calls=%fused_computation.22 | convolution fusion | flops 412483584 | bytes 10618026 | tf_op jit(solution)/shard_map/dot_general | solution.py:123
  425.4 1.6 multiply_reduce_fusion.1
  427.0 3.5 convolution_convert_fusion.1
  430.5 4.7 %all-to-all-start = ((bf16[4,64,2048]{2,1,0:T(8,128)(2,1)}), bf16[4,64,2048]{2,1,0:T(8,128)(2,1)}, u32[]{:S(2)}, u32[]{:S(2)}) async-start(bf16[4,64,2048]{2,1,0:T(8,128)(2,1)} %bitcast.67), calls=%async_computation | async-start | bytes 2097152 | tf_op jit(solution)/shard_map/all_to_all | solution.py:61
  435.3 1.5 reshape.340
  436.8 1.7 gather_fusion.1
  438.5 1.7 reshape.347
  440.2 2.2 multiply_reduce_fusion
  442.4 5.1 %all-to-all-done = bf16[4,64,2048]{2,1,0:T(8,128)(2,1)} async-done(((bf16[4,64,2048]{2,1,0:T(8,128)(2,1)}), bf16[4,64,2048]{2,1,0:T(8,128)(2,1)}, u32[]{:S(2)}, u32[]{:S(2)}) %all-to-all-start) | async-done | bytes 1048608 | tf_op jit(solution)/shard_map/all_to_all | solution.py:61
  447.5 2.2 reduce_sum.60
  (167 shorter events, 75.4 us)
Async XLA Ops:
  7.2 238.9 %copy-start = (bf16[1,512,2048]{2,1,0:T(8,128)(2,1)S(1)}, bf16[1,512,2048]{2,1,0:T(8,128)(2,1)}, u32[]{:S(2)}) copy-start(bf16[1,512,2048]{2,1,0:T(8,128)(2,1)} %param.33) | copy-start | bytes 6291460
  7.2 46.2 %copy-start.9 = (s32[64,2]{0,1:T(2,128)S(1)}, s32[64,2]{0,1:T(2,128)}, u32[]{:S(2)}) copy-start(s32[64,2]{0,1:T(2,128)} %param.29) | copy-start | bytes 1540
  7.2 47.1 %all-gather.10.cloned.1.call-start = ((), (), s32[]{:S(2)}) async-start(), calls=%async_computation.5 | async-start | bytes 1572864 | tf_op jit(solution)/shard_map/all_gather | solution.py:43
  13.8 43.8 %copy-start.1 = (bf16[64,2048]{1,0:T(8,128)(2,1)S(1)}, bf16[64,2048]{1,0:T(8,128)(2,1)}, u32[]{:S(2)}) copy-start(bf16[64,2048]{1,0:T(8,128)(2,1)} %param.27) | copy-start | bytes 786436
  13.8 256.0 %all-gather.8.cloned.1.call-start = ((), (), s32[]{:S(2)}) async-start(), calls=%async_computation.4 | async-start | bytes 17301504 | tf_op jit(solution)/shard_map/all_gather | solution.py:20
  22.4 35.5 %copy-start.8 = (f32[2048]{0:T(1024)S(1)}, f32[2048]{0:T(1024)}, u32[]{:S(2)}) copy-start(f32[2048]{0:T(1024)} %param.28) | copy-start | bytes 24580
  24.8 394.2 %all-gather.6.cloned.1.call-start = ((), (), s32[]{:S(2)}) async-start(), calls=%async_computation.3 | async-start | bytes 8912896 | tf_op jit(solution)/shard_map/all_gather | solution.py:43
  62.2 15.6 %copy-start.13 = (u32[256]{0:T(256)S(1)}, u32[256]{0:T(256)}, u32[]{:S(2)}) copy-start(u32[256]{0:T(256)} %constant.154) | copy-start | bytes 3076
  62.2 180.9 %copy-start.7 = (f32[1,256]{1,0:T(1,128)S(1)}, f32[1,256]{1,0:T(1,128)}, u32[]{:S(2)}) copy-start(f32[1,256]{1,0:T(1,128)} %param.24) | copy-start | bytes 3076
  62.2 180.9 %copy-start.10 = (f32[1,256]{1,0:T(1,128)S(1)}, f32[1,256]{1,0:T(1,128)}, u32[]{:S(2)}) copy-start(f32[1,256]{1,0:T(1,128)} %param.23) | copy-start | bytes 3076
  62.2 180.9 %copy-start.6 = (f32[1,256]{1,0:T(1,128)S(1)}, f32[1,256]{1,0:T(1,128)}, u32[]{:S(2)}) copy-start(f32[1,256]{1,0:T(1,128)} %param.22) | copy-start | bytes 3076
  65.4 178.0 %all-to-all-start.1 = ((bf16[128,1,2,2048]{3,2,1,0:T(2,128)(2,1)}), bf16[128,1,2,2048]{3,2,1,0:T(2,128)(2,1)}, u32[]{:S(2)}, u32[]{:S(2)}) async-start(bf16[128,1,2,2048]{3,2,1,0:T(2,128)(2,1)} %fusion.27), calls=%async_computation.1 | async-start | bytes 2097152 | tf_op jit(solution)/shard_map/all_to_all | solution.py:239
  253.7 176.7 %all-to-all-start.2 = ((bf16[128,1,2,2048]{3,2,1,0:T(2,128)(2,1)}), bf16[128,1,2,2048]{3,2,1,0:T(2,128)(2,1)}, u32[]{:S(2)}, u32[]{:S(2)}) async-start(bf16[128,1,2,2048]{3,2,1,0:T(2,128)(2,1)} %copy.38), calls=%async_computation.2 | async-start | bytes 2097152 | tf_op jit(solution)/shard_map/all_to_all | solution.py:250
  269.7 148.0 %copy-start.5 = (bf16[256,256]{1,0:T(8,128)(2,1)S(1)}, bf16[256,256]{1,0:T(8,128)(2,1)}, u32[]{:S(2)}) copy-start(bf16[256,256]{1,0:T(8,128)(2,1)} %param.18) | copy-start | bytes 393220
  269.8 149.3 %copy-start.2 = (f32[1,256,512]{2,1,0:T(8,128)S(1)}, f32[1,256,512]{2,1,0:T(8,128)}, u32[]{:S(2)}) copy-start(f32[1,256,512]{2,1,0:T(8,128)} %fusion.71) | copy-start | bytes 1572868
  419.0 6.4 %copy-start.3 = (bf16[256,512]{1,0:T(8,128)(2,1)S(1)}, bf16[256,512]{1,0:T(8,128)(2,1)}, u32[]{:S(2)}) copy-start(bf16[256,512]{1,0:T(8,128)(2,1)} %param.20) | copy-start | bytes 786436
  419.0 6.4 %copy-start.4 = (bf16[256,256]{1,0:T(8,128)(2,1)S(1)}, bf16[256,256]{1,0:T(8,128)(2,1)}, u32[]{:S(2)}) copy-start(bf16[256,256]{1,0:T(8,128)(2,1)} %param.19) | copy-start | bytes 393220
  419.0 7.9 %copy-start.12 = (f32[512]{0:T(512)S(1)}, f32[512]{0:T(512)}, u32[]{:S(2)}) copy-start(f32[512]{0:T(512)} %param.25) | copy-start | bytes 6148
  430.5 4.7 %copy-start.11 = (f32[64,2]{0,1:T(2,128)S(1)}, f32[64,2]{0,1:T(2,128)}, u32[]{:S(2)}) copy-start(f32[64,2]{0,1:T(2,128)} %param.30) | copy-start | bytes 1540
  430.5 17.0 %all-to-all-start = ((bf16[4,64,2048]{2,1,0:T(8,128)(2,1)}), bf16[4,64,2048]{2,1,0:T(8,128)(2,1)}, u32[]{:S(2)}, u32[]{:S(2)}) async-start(bf16[4,64,2048]{2,1,0:T(8,128)(2,1)} %bitcast.67), calls=%async_computation | async-start | bytes 2097152 | tf_op jit(solution)/shard_map/all_to_all | solution.py:61
Sparse Core Ops, SparseCore 0:
  13.9 33.6 all-gather.9
  49.4 151.0 all-gather.7
  202.3 146.8 all-gather.5
where the time goes:
time: 462 us; the launch traced here: 456 us
  blocking collectives  151 us (33%)
  local copies, waits for them, and re-layouts  65.1 us (14%)
  other arithmetic  64.7 us (14%)
  loops' own time  62.7 us (14%)
  between operations  51.7 us (11%)
  starting transfers between devices  31.9 us (7%)
  matrix products  24.3 us (5%)
  waiting for transfers between devices  5.28 us (1%)
    unnamed x3, blocking collectives  151 us
    another operation x1, loops' own time, prefix(): return lax.fori_loop(0, count - 1, lap, so_far)  62.7 us
    select_n x31, other arithmetic, lap(): jnp.where(position < mine, new, old)  45 us
    dynamic_slice x62, local copies, waits for them, and re-layouts, lap(): longer = join(so_far, jax.tree.map(lambda part: part[position], pieces))  39.6 us
    all_to_all x1, starting transfers between devices, expert_part(): lax.all_to_all(results, EP_TP, split_axis=0, concat_axis=0, tiled=True)  16 us
    all_to_all x1, starting transfers between devices, expert_part(): lax.all_to_all(outgoing.reshape(devices, local_experts, capacity, model_w...  11 us
    unnamed x44, local copies, waits for them, and re-layouts  9.76 us
  transfers between devices with their start and end apart: 6, of which 1 were waited for; matrix products, arithmetic and copies ran while one was open for 32% of the time, Pallas kernels for 0%

commit v1 on v0

v1 whole, which is shorter than its diff:
```python
import functools
import math

import jax
import jax.numpy as jnp
from jax import lax
from jax.experimental import pallas as pl
from jax.experimental.pallas import tpu as pltpu
from jax.sharding import PartitionSpec as P

MESH = pl.DeviceIdType.MESH
F32 = jnp.float32
BF16 = jnp.bfloat16

GRP_EP = ("grp", "ep")
GRP_EP_TP = ("grp", "ep", "tp")
EP_TP = ("ep", "tp")

lowest_log = -1e30
norm_eps = 1e-06
layer_eps = 1e-05
cap = 2
cores = 2


def mm(a, b):
    return lax.dot_general(a, b, (((1,), (0,)), ((), ())), preferred_element_type=F32)


def mm_t(a, b):
    return lax.dot_general(a, b, (((1,), (1,)), ((), ())), preferred_element_type=F32)


def mm_split(a, b):
    high = a.astype(BF16)
    low = (a - high.astype(F32)).astype(BF16)
    return mm(high, b) + mm(low, b)


def iota(shape, dim):
    return lax.broadcasted_iota(jnp.int32, shape, dim)


def kernel(
    nz,
    nx,
    groups,
    q_ref,
    k_ref,
    v_ref,
    og_ref,
    in_gate_ref,
    forget_ref,
    extra_ref,
    head_gain_ref,
    tok_ref,
    norm_gain_ref,
    routes_ref,
    weight_ref,
    wout_hbm,
    wg_hbm,
    wu_hbm,
    wd_hbm,
    mix_ref,
    exp_ref,
    wout,
    wg,
    wu,
    wd,
    normed,
    out1,
    in1,
    out2,
    in2,
    hidden,
    res,
    back,
    ret_out,
    ret_in,
    own_state,
    state_out,
    state_in,
    stat_out,
    stat_in,
    chip_state,
    chip_in,
    chip_stat,
    stats,
    scan_out,
    far,
    gated,
    head_part,
    parts_in,
    load_sem,
    pair_s,
    pair_r,
    z_s,
    z_r,
    x_s,
    x_r,
    a_s,
    a_r,
    t_s,
    t_r,
    b_s,
    b_r,
    rs_s,
    rs_r,
    xb_s,
    xb_r,
    zb_s,
    zb_r,
):
    ep = lax.axis_index("ep")
    x = lax.axis_index("tp")
    z = ep // cores
    c = ep % cores
    nr = nx * cores
    r = c * nx + x
    blk = nr * cap
    gs = nz // groups
    half = nz // 2
    tokens, width = tok_ref.shape
    span, dqk = q_ref.shape
    dv = v_ref.shape[1]
    tile = min(512, width)
    hr = dqk // 2 // nz

    def at(z_, c_, x_):
        return {"ep": z_ * cores + c_, "tp": x_}

    def row_dev(r_):
        return at(z, r_ // nx, r_ % nx)

    def offset(p):
        return half - (p + 1) // 2 if p % 2 else (half + p // 2) % nz if p < nz - 1 else 0

    def copy(src, dst, ssem, rsem, dev):
        return pltpu.make_async_remote_copy(
            src_ref=src,
            dst_ref=dst,
            send_sem=ssem,
            recv_sem=rsem,
            device_id=dev,
            device_id_type=MESH,
        )

    loads = [
        pltpu.make_async_copy(wg_hbm.at[0], wg, load_sem.at[0]),
        pltpu.make_async_copy(wu_hbm.at[0], wu, load_sem.at[1]),
        pltpu.make_async_copy(wd_hbm.at[0], wd, load_sem.at[2]),
        pltpu.make_async_copy(wout_hbm, wout, load_sem.at[3]),
    ]
    for load in loads:
        load.start()

    barrier = pltpu.get_barrier_semaphore()
    for i in range(1, nz):
        pl.semaphore_signal(
            barrier, inc=1, device_id=at((z + i) % nz, c, x), device_id_type=MESH
        )
    for i in range(1, nr):
        pl.semaphore_signal(barrier, inc=1, device_id=row_dev((r + i) % nr), device_id_type=MESH)

    t_f32 = tok_ref[...].astype(F32)
    centre = jnp.mean(t_f32, axis=1, keepdims=True)
    t_f32 = t_f32 - centre
    spread = jnp.mean(t_f32 * t_f32, axis=1, keepdims=True)
    normed[...] = (t_f32 * lax.rsqrt(spread + layer_eps) * norm_gain_ref[...]).astype(BF16)

    t0 = iota((tokens, tokens), 0)
    t1 = iota((tokens, tokens), 1)
    e_col = [routes_ref[:, k : k + 1].astype(F32) for k in range(2)]
    e_row = [jnp.sum(jnp.where(t0 == t1, e, 0.0), axis=0, keepdims=True) for e in e_col]

    def place(e, earlier):
        e = e.astype(jnp.int32)
        step = ((e >> int(math.log2(nr))) - z) & (nz - 1)
        p = jnp.where(step < half, 2 * (half - step) - 1, 2 * (step - half))
        return p * blk + (e & (nr - 1)) * cap + earlier.astype(jnp.int32)

    def one_if(mask):
        return jnp.where(mask, 1.0, 0.0)

    place_row, place_col = [], []
    for k in range(2):
        same = (e_col[0] == e_row[k]) | (e_col[1] == e_row[k])
        earlier = jnp.sum(one_if(same & (t0 < t1)), axis=0, keepdims=True)
        place_row.append(place(e_row[k], earlier))
        same = (e_row[0] == e_col[k]) | (e_row[1] == e_col[k])
        earlier = jnp.sum(one_if(same & (t1 < t0)), axis=1, keepdims=True)
        place_col.append(place(e_col[k], earlier))
    rows = iota((nz * blk, tokens), 0)
    pick = one_if((rows == place_row[0]) | (rows == place_row[1])).astype(BF16)
    for n in range(0, width, tile):
        out1[:, :, n : n + tile] = (
            mm(pick, normed[:, n : n + tile]).astype(BF16).reshape(nz, blk, tile)
        )

    pl.semaphore_wait(barrier, nz - 1 + nr - 1)

    sends = []

    def send(*args):
        made = copy(*args)
        made.start()
        sends.append(made)
        return made

    z_copies = [
        send(
            out1.at[p],
            in1.at[p],
            z_s.at[p],
            z_r.at[p],
            at((z + offset(p)) % nz, c, x),
        )
        for p in range(nz - 1)
    ]
    in1[nz - 1] = out1[nz - 1]

    forget = forget_ref[...]
    forget = jnp.minimum(forget, 0.0) - jnp.log1p(jnp.exp(-jnp.abs(forget))) + extra_ref[...]
    in_gate = in_gate_ref[...]
    ti = iota((span, span), 0)
    si = iota((span, span), 1)
    forget_col = jnp.sum(jnp.where(ti == si, forget, 0.0), axis=1, keepdims=True)
    through_row = jnp.sum(jnp.where(ti <= si, forget_col, 0.0), axis=0, keepdims=True)
    through_col = jnp.sum(jnp.where(si <= ti, forget, 0.0), axis=1, keepdims=True)
    before_row = through_row - forget
    before_col = through_col - forget_col
    total = jnp.sum(forget, axis=1, keepdims=True)
    fw_log = total - through_row + in_gate
    bw_log = before_row + in_gate
    fw_top = jnp.max(fw_log, axis=1, keepdims=True)
    bw_top = jnp.max(bw_log, axis=1, keepdims=True)
    keys_t = jnp.transpose(k_ref[...].astype(F32))
    values = v_ref[...]
    own_state[0] = mm_split(keys_t * jnp.exp(fw_log - fw_top), values)
    own_state[1] = mm_split(keys_t * jnp.exp(bw_log - bw_top), values)
    state_out[...] = own_state[...].astype(BF16)
    stat_out[0:1, :] = jnp.broadcast_to(fw_top, (1, 128))
    stat_out[1:2, :] = jnp.broadcast_to(bw_top, (1, 128))
    stat_out[2:3, :] = jnp.broadcast_to(total, (1, 128))
    stat_out[3:8, :] = jnp.zeros((5, 128), F32)
    partner = at(z, 1 - c, x)
    pair_copies = [
        send(state_out, state_in, pair_s.at[0], pair_r.at[0], partner),
        send(stat_out, stat_in, pair_s.at[1], pair_r.at[1], partner),
    ]

    scale = dqk**-0.5
    fw_in = jnp.where(ti >= si, through_col - through_row + in_gate, -jnp.inf)
    bw_in = jnp.where(ti <= si, before_row - before_col + in_gate, -jnp.inf)
    inner_top = jnp.maximum(
        jnp.max(fw_in, axis=1, keepdims=True), jnp.max(bw_in, axis=1, keepdims=True)
    )

    for made in pair_copies:
        made.wait_recv()
    first = c == 0

    def row(ref, i):
        return ref[i : i + 1, :]

    f_own, b_own, t_own = (row(stat_out, i) for i in range(3))
    f_par, b_par, t_par = (row(stat_in, i) for i in range(3))
    f_own_log = f_own + jnp.where(first, t_par, 0.0)
    f_par_log = f_par + jnp.where(first, 0.0, t_own)
    b_own_log = b_own + jnp.where(first, 0.0, t_par)
    b_par_log = b_par + jnp.where(first, t_own, 0.0)
    f_chip = jnp.maximum(f_own_log, f_par_log)
    b_chip = jnp.maximum(b_own_log, b_par_log)
    mine = pl.ds(pl.multiple_of(c * (dqk // 2), dqk // 2), dqk // 2)
    for i, (own_log, par_log, top) in enumerate(
        ((f_own_log, f_par_log, f_chip), (b_own_log, b_par_log, b_chip))
    ):
        joined = (
            jnp.exp(own_log - top)[:, 0:1] * own_state[i, mine, :]
            + jnp.exp(par_log - top)[:, 0:1] * state_in[i, mine, :].astype(F32)
        )
        chip_state[:, i * hr : (i + 1) * hr, :] = joined.astype(BF16).reshape(nz, hr, dv)
    chip_stat[0:1, :] = f_chip
    chip_stat[1:2, :] = b_chip
    chip_stat[2:3, :] = t_own + t_par
    chip_stat[3:8, :] = jnp.zeros((5, 128), F32)
    a_copies = []
    for i in range(1, nz):
        to = (z + i) % nz
        dev = at(to, c, x)
        a_copies.append(send(chip_stat, stats.at[z], t_s.at[i], t_r.at[i], dev))
        a_copies.append(send(chip_state.at[to], chip_in.at[z], a_s.at[i], a_r.at[i], dev))
    chip_in[z] = chip_state[z]
    stats[z] = chip_stat[...]

    ga, gb = iota((gs * blk, gs * blk), 0), iota((gs * blk, gs * blk), 1)
    lc, lg, lr = (int(math.log2(n)) for n in (cap, gs, nr))
    to_row = ga >> (lc + lg)
    to_mem = (ga >> lc) & (gs - 1)
    fwd = one_if(gb == to_mem * blk + to_row * cap + (ga & (cap - 1))).astype(BF16)
    from_mem = ga >> (lc + lr)
    from_row = (ga >> lc) & (nr - 1)
    rev = one_if(gb == from_row * (gs * cap) + from_mem * cap + (ga & (cap - 1))).astype(BF16)

    x_copies = []
    for g in range(groups):
        for p in range(g * gs, min((g + 1) * gs, nz - 1)):
            z_copies[p].wait_recv()
        for n in range(0, width, tile):
            rows_in = in1[g * gs : (g + 1) * gs, :, n : n + tile].reshape(gs * blk, tile)
            out2[g, :, :, n : n + tile] = (
                mm(fwd, rows_in).astype(BF16).reshape(nr, gs * cap, tile)
            )
        for i in range(1, nr):
            to = (r + i) % nr
            x_copies.append(
                send(out2.at[g, to], in2.at[g, i], x_s.at[g, i], x_r.at[g, i], row_dev(to))
            )
        in2[g, 0] = out2[g, r]

    loads[0].wait()
    loads[1].wait()
    loads[2].wait()
    for made in x_copies:
        made.wait_recv()
    n_rows = nz * blk
    fe = wg.shape[1]
    ft = min(256, fe)
    for n in range(0, fe, ft):
        arrived = in2[...].reshape(n_rows, width)
        gate_part = mm(arrived, wg[:, n : n + ft])
        up_part = mm(arrived, wu[:, n : n + ft])
        hidden[:, n : n + ft] = (gate_part * jax.nn.sigmoid(gate_part) * up_part).astype(BF16)
    for n in range(0, width, tile):
        res[:, :, :, n : n + tile] = (
            mm(hidden[...], wd[:, n : n + tile]).astype(BF16).reshape(groups, nr, gs * cap, tile)
        )
    xb_copies = []
    for g in range(groups):
        made = []
        for i in range(1, nr):
            to = (r + nr - i) % nr
            made.append(
                send(res.at[g, i], back.at[g, r], xb_s.at[g, i], xb_r.at[g, i], row_dev(to))
            )
        xb_copies.append(made)
        back[g, r] = res[g, 0]

    for made in a_copies:
        made.wait_recv()
    lanes = [pl.ds(n, 128) for n in range(0, dv, 128)]
    tops = []
    for i, order in ((0, range(nz)), (1, range(nz - 1, -1, -1))):
        top = jnp.full((1, 128), lowest_log, F32)
        my_top = top
        memory = [jnp.zeros((hr, 128), F32) for _ in lanes]
        for w in order:
            my_top = jnp.where(w == z, top, my_top)
            for lane, m in zip(lanes, memory):
                scan_out[w, i * hr : (i + 1) * hr, lane] = m.astype(BF16)
            state_top, state_total = stats[w, i : i + 1, :], stats[w, 2:3, :]
            new_top = jnp.maximum(state_total + top, state_top)
            keep = jnp.exp(state_total + top - new_top)
            take = jnp.exp(state_top - new_top)
            memory = [
                keep * m + take * chip_in[w, i * hr : (i + 1) * hr, lane].astype(F32)
                for lane, m in zip(lanes, memory)
            ]
            top = new_top
        tops.append(my_top[:, 0:1])
    b_copies = []
    for i in range(1, nz):
        to = (z + i) % nz
        b_copies.append(
            send(scan_out.at[to], far.at[c, z], b_s.at[i], b_r.at[i], at(to, c, x))
        )
    far[c, z] = scan_out[z]

    zb_copies = []
    for g in range(groups):
        for made in xb_copies[g]:
            made.wait_recv()
        for n in range(0, width, tile):
            rows_in = back[g, :, :, n : n + tile].reshape(gs * blk, tile)
            ret_out[g * gs : (g + 1) * gs, :, n : n + tile] = (
                mm(rev, rows_in).astype(BF16).reshape(gs, blk, tile)
            )
        for p in range(g * gs, min((g + 1) * gs, nz - 1)):
            zb_copies.append(
                send(
                    ret_out.at[p],
                    ret_in.at[p],
                    zb_s.at[p],
                    zb_r.at[p],
                    at((z + nz - offset(p)) % nz, c, x),
                )
            )
    ret_in[nz - 1] = ret_out[nz - 1]

    for made in b_copies:
        made.wait_recv()
    far_copy = send(far.at[c], far.at[c], pair_s.at[2], pair_r.at[2], partner)
    far_in = copy(far.at[c], far.at[1 - c], pair_s.at[2], pair_r.at[2], partner)
    scores = mm_t(q_ref[...], k_ref[...]) * scale
    t_own, t_par, f_par, b_par = (v[:, 0:1] for v in (t_own, t_par, f_par, b_par))
    rest_col = total - before_col
    prior_log = through_col + (tops[0] + jnp.where(first, 0.0, t_par))
    later_log = rest_col + (tops[1] + jnp.where(first, t_par, 0.0))
    pair_log = jnp.where(first, rest_col + b_par, through_col + f_par)
    row_top = jnp.maximum(
        jnp.maximum(inner_top, prior_log), jnp.maximum(later_log, pair_log)
    )
    weights = jnp.exp(fw_in - row_top) + jnp.exp(bw_in - row_top)
    near = (scores * weights).astype(BF16)
    far_in.wait_recv()
    queries = q_ref[...]

    def far_memory(i):
        return far[:, :, i * hr : (i + 1) * hr, :].reshape(dqk, dv)

    head_rows = mm(near, v_ref[...]) + scale * (
        jnp.exp(prior_log - row_top) * mm(queries, far_memory(0))
        + jnp.exp(later_log - row_top) * mm(queries, far_memory(1))
        + jnp.exp(pair_log - row_top) * mm(queries, state_in[1 - c])
    )
    head_rows = (
        head_rows
        * lax.rsqrt(jnp.mean(head_rows * head_rows, axis=1, keepdims=True) + norm_eps)
        * head_gain_ref[...]
    )
    gated[...] = (jax.nn.sigmoid(og_ref[...].astype(F32)) * head_rows).astype(BF16)
    loads[3].wait()
    for n in range(0, width, tile):
        head_part[:, :, n : n + tile] = (
            mm(gated[...], wout[:, n : n + tile]).astype(BF16).reshape(nx, span // nx, tile)
        )
    rs_copies = []
    for i in range(1, nx):
        to = (x + i) % nx
        rs_copies.append(
            send(head_part.at[to], parts_in.at[i], rs_s.at[i], rs_r.at[i], at(z, c, to))
        )
    for made in rs_copies:
        made.wait_recv()
    for n in range(0, width, tile):
        mixed = head_part[x, :, n : n + tile].astype(F32)
        for i in range(1, nx):
            mixed = mixed + parts_in[i, :, n : n + tile].astype(F32)
        mix_ref[:, n : n + tile] = mixed.astype(BF16)

    places = iota((tokens, nz * blk), 1)
    share = jnp.where(places == place_col[0], weight_ref[:, 0:1], 0.0) + jnp.where(
        places == place_col[1], weight_ref[:, 1:2], 0.0
    )
    for made in zb_copies:
        made.wait_recv()
    for n in range(0, width, tile):
        returned = ret_in[:, :, n : n + tile].reshape(nz * blk, tile)
        exp_ref[:, n : n + tile] = mm_split(share, returned).astype(BF16)

    for made in sends:
        made.wait_send()


def body(
    nz,
    nx,
    queries,
    head_key_rows,
    head_value_rows,
    output_gate_logits,
    log_input_gate,
    forget_gate_logits,
    extra_log_forget,
    head_norm_gain,
    memory_output_matrix,
    expert_input_tokens,
    expert_norm_gain,
    routes,
    routed_expert_weight,
    expert_gate_matrix,
    expert_up_matrix,
    expert_down_matrix,
):
    span, dqk = queries.shape
    dv = head_value_rows.shape[1]
    tokens, width = expert_input_tokens.shape
    fe = expert_gate_matrix.shape[2]
    nr = nx * cores
    blk = nr * cap
    groups = 4 if nz % 4 == 0 else 1
    gs = nz // groups
    hr = dqk // 2 // nz
    vmem = pl.BlockSpec(memory_space=pltpu.VMEM)
    hbm = pl.BlockSpec(memory_space=pl.ANY)
    dma = pltpu.SemaphoreType.DMA
    mixer_out, expert_out = pl.pallas_call(
        functools.partial(kernel, nz, nx, groups),
        out_shape=(
            jax.ShapeDtypeStruct((span // nx, width), BF16),
            jax.ShapeDtypeStruct((tokens, width), BF16),
        ),
        in_specs=[vmem] * 12 + [hbm] * 4,
        out_specs=(vmem, vmem),
        scratch_shapes=[
            pltpu.VMEM((dv, width), BF16),
            pltpu.VMEM((width, fe), BF16),
            pltpu.VMEM((width, fe), BF16),
            pltpu.VMEM((fe, width), BF16),
            pltpu.VMEM((tokens, width), BF16),
            pltpu.VMEM((nz, blk, width), BF16),
            pltpu.VMEM((nz, blk, width), BF16),
            pltpu.VMEM((groups, nr, gs * cap, width), BF16),
            pltpu.VMEM((groups, nr, gs * cap, width), BF16),
            pltpu.VMEM((nz * blk, fe), BF16),
            pltpu.VMEM((groups, nr, gs * cap, width), BF16),
            pltpu.VMEM((groups, nr, gs * cap, width), BF16),
            pltpu.VMEM((nz, blk, width), BF16),
            pltpu.VMEM((nz, blk, width), BF16),
            pltpu.VMEM((2, dqk, dv), F32),
            pltpu.VMEM((2, dqk, dv), BF16),
            pltpu.VMEM((2, dqk, dv), BF16),
            pltpu.VMEM((8, 128), F32),
            pltpu.VMEM((8, 128), F32),
            pltpu.VMEM((nz, 2 * hr, dv), BF16),
            pltpu.VMEM((nz, 2 * hr, dv), BF16),
            pltpu.VMEM((8, 128), F32),
            pltpu.VMEM((nz, 8, 128), F32),
            pltpu.VMEM((nz, 2 * hr, dv), BF16),
            pltpu.VMEM((2, nz, 2 * hr, dv), BF16),
            pltpu.VMEM((span, dv), BF16),
            pltpu.VMEM((nx, span // nx, width), BF16),
            pltpu.VMEM((nx, span // nx, width), BF16),
            dma((4,)),
            dma((3,)),
            dma((3,)),
            dma((nz,)),
            dma((nz,)),
            dma((groups, nr)),
            dma((groups, nr)),
            dma((nz,)),
            dma((nz,)),
            dma((nz,)),
            dma((nz,)),
            dma((nz,)),
            dma((nz,)),
            dma((nx,)),
            dma((nx,)),
            dma((groups, nr)),
            dma((groups, nr)),
            dma((nz,)),
            dma((nz,)),
        ],
        compiler_params=pltpu.CompilerParams(
            collective_id=0, has_side_effects=True, vmem_limit_bytes=60 * 2**20
        ),
        name="layer_step",
    )(
        queries,
        head_key_rows,
        head_value_rows,
        output_gate_logits,
        log_input_gate,
        forget_gate_logits,
        extra_log_forget,
        head_norm_gain.reshape(1, dv),
        expert_input_tokens,
        expert_norm_gain.reshape(1, width),
        routes,
        routed_expert_weight,
        memory_output_matrix,
        expert_gate_matrix,
        expert_up_matrix,
        expert_down_matrix,
    )
    return mixer_out, expert_out


def solution(mesh):
    nz = mesh.shape["ep"] // cores
    return jax.shard_map(
        functools.partial(body, nz, mesh.shape["tp"]),
        mesh=mesh,
        in_specs=(
            P(GRP_EP, "tp"),
            P(GRP_EP, "tp"),
            P(GRP_EP, "tp"),
            P(GRP_EP, "tp"),
            P("tp", GRP_EP),
            P("tp", GRP_EP),
            P("tp", GRP_EP),
            P("tp"),
            P("tp", None),
            P(GRP_EP_TP, None),
            P(),
            P(GRP_EP_TP, None),
            P(GRP_EP_TP, None),
            P(EP_TP, None, None),
            P(EP_TP, None, None),
            P(EP_TP, None, None),
        ),
        out_specs=(P(GRP_EP_TP, None), P(GRP_EP_TP, None)),
        check_vma=False,
    )
```

time: 462 us -> 161 us (0.35); the launches traced: 456 us -> 161 us
  Pallas kernels: 0 us -> 155 us
  blocking collectives: 151 us -> 0 us
  other arithmetic: 64.7 us -> 0 us
  loops' own time: 62.7 us -> 0 us
  local copies, waits for them, and re-layouts: 65.1 us -> 6.1 us
  between operations: 51.7 us -> 0.64 us
  starting transfers between devices: 31.9 us -> 0 us
  matrix products: 24.3 us -> 0 us
  waiting for transfers between devices: 5.28 us -> 0 us
    pallas_call x0 -> x1, Pallas kernels: none -> 155 us  [body(): pl.pallas_call(functools.partial(kernel, nz, nx, groups), out_shape=(jax....]
    unnamed x3 -> x0, blocking collectives: 151 us -> none
    another operation x1 -> x0, loops' own time: 62.7 us -> none  [prefix(): return lax.fori_loop(0, count - 1, lap, so_far)]
    select_n x35 -> x0, other arithmetic: 48.3 us -> none  [the longest x31 45 us: lap(): jnp.where(position < mine, new, old)]
    dynamic_slice x62 -> x0, local copies, waits for them, and re-layouts: 39.6 us -> none  [lap(): longer = join(so_far, jax.tree.map(lambda part: part[position], pieces))]
    all_to_all x3 -> x0, starting transfers between devices: 31.7 us -> none  [the longest x1 16 us: expert_part(): lax.all_to_all(results, EP_TP, split_axis=0, concat_axis=0, tiled=True)]
    dot_general x8 -> x0, matrix products: 24.3 us -> none  [the longest x1 6.34 us: block_output(): jnp.dot(queries_f32, later_memory, precision=lax.Precision.HIGHEST)]
    all_to_all x3 -> x0, waiting for transfers between devices: 5.08 us -> none  [the longest x1 5.07 us: summed_on_arrival(): lax.all_to_all(blocks, axis, split_axis=0, concat_axis=0, tiled=True)]
  transfers between devices with their start and end apart: 6 -> 0, of which waited for: 1 -> 0; matrix products, arithmetic and copies ran while one was open for 32% -> 0% of each run, Pallas kernels for 0% -> 0%
where the time goes in v1:
time: 161 us
  Pallas kernels  155 us (96%)
  local copies, waits for them, and re-layouts  6.1 us (4%)
    pallas_call x1, Pallas kernels, body(): pl.pallas_call(functools.partial(kernel, nz, nx, groups), out_shape=(jax....  155 us
    unnamed x4, local copies, waits for them, and re-layouts  6.1 us

profile of v1, /device:TPU:33, one launch (start us, length us, event | category | flops | bytes accessed | tf_op | source)
XLA Modules:
  0.0 161.3 jit_solution(6475704180447699097)
XLA Ops:
  0.6 1.4 copy.18.routes_ref
  2.0 1.4 copy.19.weight_ref
  3.4 154.5 %layer_step.1 = (bf16[64,2048]{1,0:T(8,128)(2,1)}, bf16[64,2048]{1,0:T(8,128)(2,1)}) custom-call(bf16[256,256]{1,0:T(8,128)(2,1)} %q_ref.1, bf16[256,256]{1,0:T(8,128)(2,1)} %k_ref.1, bf16[256,512]{1,0:T(8,128)(2,1)} %v_ref.1, bf16[256,512]{1,0:T(8,128)(2,1)} %og_ref.1, f32[1,256]{1,0:T(1,128)} %in_gate_ref.1, f32[1,256]{1,0:T(1,128)} %forget_ref.1, ...), custom_call_target="tpu_custom_call" | custom-call | tf_op jit(solution)/shard_map/layer_step/pallas_call | solution.py:497
  157.9 1.7 %copy.22 = bf16[64,2048]{1,0:T(8,128)(2,1)} copy(bf16[64,2048]{1,0:T(8,128)(2,1)} %get-tuple-element.4) | data formatting | bytes 524288
  159.6 1.7 %copy.23 = bf16[64,2048]{1,0:T(8,128)(2,1)} copy(bf16[64,2048]{1,0:T(8,128)(2,1)} %get-tuple-element.5) | data formatting | bytes 524288

commit v2 on v1

--- a/solution.py
+++ b/solution.py
@@ -170,8 +170,12 @@
 
     t0 = iota((tokens, tokens), 0)
     t1 = iota((tokens, tokens), 1)
-    e_col = [routes_ref[:, k : k + 1].astype(F32) for k in range(2)]
-    e_row = [jnp.sum(jnp.where(t0 == t1, e, 0.0), axis=0, keepdims=True) for e in e_col]
+
+    def to_col(row):
+        return jnp.sum(jnp.where(t0 == t1, row, 0.0), axis=1, keepdims=True)
+
+    e_row = [routes_ref[k : k + 1, :].astype(F32) for k in range(2)]
+    e_col = [to_col(e) for e in e_row]
 
     def place(e, earlier):
         e = e.astype(jnp.int32)
@@ -207,16 +211,19 @@
         sends.append(made)
         return made
 
-    z_copies = [
-        send(
-            out1.at[p],
-            in1.at[p],
-            z_s.at[p],
-            z_r.at[p],
-            at((z + offset(p)) % nz, c, x),
-        )
-        for p in range(nz - 1)
-    ]
+    def z_send(places):
+        return [
+            send(
+                out1.at[p],
+                in1.at[p],
+                z_s.at[p],
+                z_r.at[p],
+                at((z + offset(p)) % nz, c, x),
+            )
+            for p in places
+        ]
+
+    z_copies = z_send(range(min(gs, nz - 1)))
     in1[nz - 1] = out1[nz - 1]
 
     forget = forget_ref[...]
@@ -290,6 +297,7 @@
         dev = at(to, c, x)
         a_copies.append(send(chip_stat, stats.at[z], t_s.at[i], t_r.at[i], dev))
         a_copies.append(send(chip_state.at[to], chip_in.at[z], a_s.at[i], a_r.at[i], dev))
+    z_copies += z_send(range(min(gs, nz - 1), nz - 1))
     chip_in[z] = chip_state[z]
     stats[z] = chip_stat[...]
 
@@ -302,41 +310,40 @@
     from_row = (ga >> lc) & (nr - 1)
     rev = one_if(gb == from_row * (gs * cap) + from_mem * cap + (ga & (cap - 1))).astype(BF16)
 
-    x_copies = []
-    for g in range(groups):
+    x_copies, xb_copies, zb_copies = [], [], []
+    n_rows = gs * blk
+    fe = wg.shape[1]
+    ft = min(256, fe)
+
+    def spread(g):
         for p in range(g * gs, min((g + 1) * gs, nz - 1)):
             z_copies[p].wait_recv()
         for n in range(0, width, tile):
-            rows_in = in1[g * gs : (g + 1) * gs, :, n : n + tile].reshape(gs * blk, tile)
+            rows_in = in1[g * gs : (g + 1) * gs, :, n : n + tile].reshape(n_rows, tile)
             out2[g, :, :, n : n + tile] = (
                 mm(fwd, rows_in).astype(BF16).reshape(nr, gs * cap, tile)
             )
+        made = []
         for i in range(1, nr):
             to = (r + i) % nr
-            x_copies.append(
+            made.append(
                 send(out2.at[g, to], in2.at[g, i], x_s.at[g, i], x_r.at[g, i], row_dev(to))
             )
+        x_copies.append(made)
         in2[g, 0] = out2[g, r]
 
-    loads[0].wait()
-    loads[1].wait()
-    loads[2].wait()
-    for made in x_copies:
-        made.wait_recv()
-    n_rows = nz * blk
-    fe = wg.shape[1]
-    ft = min(256, fe)
-    for n in range(0, fe, ft):
-        arrived = in2[...].reshape(n_rows, width)
-        gate_part = mm(arrived, wg[:, n : n + ft])
-        up_part = mm(arrived, wu[:, n : n + ft])
-        hidden[:, n : n + ft] = (gate_part * jax.nn.sigmoid(gate_part) * up_part).astype(BF16)
-    for n in range(0, width, tile):
-        res[:, :, :, n : n + tile] = (
-            mm(hidden[...], wd[:, n : n + tile]).astype(BF16).reshape(groups, nr, gs * cap, tile)
-        )
-    xb_copies = []
-    for g in range(groups):
+    def experts(g):
+        for made in x_copies[g]:
+            made.wait_recv()
+        for n in range(0, fe, ft):
+            arrived = in2[g].reshape(n_rows, width)
+            gate_part = mm(arrived, wg[:, n : n + ft])
+            up_part = mm(arrived, wu[:, n : n + ft])
+            hidden[:, n : n + ft] = (gate_part * jax.nn.sigmoid(gate_part) * up_part).astype(BF16)
+        for n in range(0, width, tile):
+            res[g, :, :, n : n + tile] = (
+                mm(hidden[...], wd[:, n : n + tile]).astype(BF16).reshape(nr, gs * cap, tile)
+            )
         made = []
         for i in range(1, nr):
             to = (r + nr - i) % nr
@@ -345,6 +352,27 @@
             )
         xb_copies.append(made)
         back[g, r] = res[g, 0]
+
+    def give_back(g):
+        for made in xb_copies[g]:
+            made.wait_recv()
+        for n in range(0, width, tile):
+            rows_in = back[g, :, :, n : n + tile].reshape(n_rows, tile)
+            ret_out[g * gs : (g + 1) * gs, :, n : n + tile] = (
+                mm(rev, rows_in).astype(BF16).reshape(gs, blk, tile)
+            )
+        for p in range(g * gs, min((g + 1) * gs, nz - 1)):
+            zb_copies.append(
+                send(
+                    ret_out.at[p],
+                    ret_in.at[p],
+                    zb_s.at[p],
+                    zb_r.at[p],
+                    at((z + nz - offset(p)) % nz, c, x),
+                )
+            )
+
+    spread(0)
 
     for made in a_copies:
         made.wait_recv()
@@ -376,25 +404,15 @@
         )
     far[c, z] = scan_out[z]
 
-    zb_copies = []
-    for g in range(groups):
-        for made in xb_copies[g]:
-            made.wait_recv()
-        for n in range(0, width, tile):
-            rows_in = back[g, :, :, n : n + tile].reshape(gs * blk, tile)
-            ret_out[g * gs : (g + 1) * gs, :, n : n + tile] = (
-                mm(rev, rows_in).astype(BF16).reshape(gs, blk, tile)
-            )
-        for p in range(g * gs, min((g + 1) * gs, nz - 1)):
-            zb_copies.append(
-                send(
-                    ret_out.at[p],
-                    ret_in.at[p],
-                    zb_s.at[p],
-                    zb_r.at[p],
-                    at((z + nz - offset(p)) % nz, c, x),
-                )
-            )
+    for load in loads[:3]:
+        load.wait()
+    for g in range(1, groups + 2):
+        if g < groups:
+            spread(g)
+        if 0 <= g - 1 < groups:
+            experts(g - 1)
+        if 0 <= g - 2 < groups:
+            give_back(g - 2)
     ret_in[nz - 1] = ret_out[nz - 1]
 
     for made in b_copies:
@@ -449,8 +467,8 @@
         mix_ref[:, n : n + tile] = mixed.astype(BF16)
 
     places = iota((tokens, nz * blk), 1)
-    share = jnp.where(places == place_col[0], weight_ref[:, 0:1], 0.0) + jnp.where(
-        places == place_col[1], weight_ref[:, 1:2], 0.0
+    share = jnp.where(places == place_col[0], to_col(weight_ref[0:1, :]), 0.0) + jnp.where(
+        places == place_col[1], to_col(weight_ref[1:2, :]), 0.0
     )
     for made in zb_copies:
         made.wait_recv()
@@ -512,7 +530,7 @@
             pltpu.VMEM((nz, blk, width), BF16),
             pltpu.VMEM((groups, nr, gs * cap, width), BF16),
             pltpu.VMEM((groups, nr, gs * cap, width), BF16),
-            pltpu.VMEM((nz * blk, fe), BF16),
+            pltpu.VMEM((gs * blk, fe), BF16),
             pltpu.VMEM((groups, nr, gs * cap, width), BF16),
             pltpu.VMEM((groups, nr, gs * cap, width), BF16),
             pltpu.VMEM((nz, blk, width), BF16),
@@ -566,8 +584,8 @@
         head_norm_gain.reshape(1, dv),
         expert_input_tokens,
         expert_norm_gain.reshape(1, width),
-        routes,
-        routed_expert_weight,
+        routes.T,
+        routed_expert_weight.T,
         memory_output_matrix,
         expert_gate_matrix,
         expert_up_matrix,

time: 161 us -> 152 us (0.944)
  Pallas kernels: 155 us -> 148 us
  local copies, waits for them, and re-layouts: 6.1 us -> 3.34 us
    pallas_call x1, Pallas kernels: 155 us -> 148 us  [body(): pl.pallas_call(functools.partial(kernel, nz, nx, groups), out_shape=(jax....]
    unnamed x4 -> x2, local copies, waits for them, and re-layouts: 6.1 us -> 3.34 us
where the time goes in v2:
time: 152 us
  Pallas kernels  148 us (97%)
  local copies, waits for them, and re-layouts  3.34 us (2%)
    pallas_call x1, Pallas kernels, body(): pl.pallas_call(functools.partial(kernel, nz, nx, groups), out_shape=(jax....  148 us
    unnamed x2, local copies, waits for them, and re-layouts  3.34 us

profile of v2, /device:TPU:33, one launch (start us, length us, event | category | flops | bytes accessed | tf_op | source)
XLA Modules:
  0.0 152.0 jit_solution(7811746493898838363)
XLA Ops:
  0.6 148.1 %layer_step.1 = (bf16[64,2048]{1,0:T(8,128)(2,1)}, bf16[64,2048]{1,0:T(8,128)(2,1)}) custom-call(bf16[256,256]{1,0:T(8,128)(2,1)} %q_ref.1, bf16[256,256]{1,0:T(8,128)(2,1)} %k_ref.1, bf16[256,512]{1,0:T(8,128)(2,1)} %v_ref.1, bf16[256,512]{1,0:T(8,128)(2,1)} %og_ref.1, f32[1,256]{1,0:T(1,128)} %in_gate_ref.1, f32[1,256]{1,0:T(1,128)} %forget_ref.1, ...), custom_call_target="tpu_custom_call" | custom-call | tf_op jit(solution)/shard_map/layer_step/pallas_call | solution.py:515
  148.7 1.7 %copy.20 = bf16[64,2048]{1,0:T(8,128)(2,1)} copy(bf16[64,2048]{1,0:T(8,128)(2,1)} %get-tuple-element.4) | data formatting | bytes 524288
  150.4 1.7 %copy.21 = bf16[64,2048]{1,0:T(8,128)(2,1)} copy(bf16[64,2048]{1,0:T(8,128)(2,1)} %get-tuple-element.5) | data formatting | bytes 524288

commit v3 on v2

--- a/solution.py
+++ b/solution.py
@@ -45,24 +45,36 @@
     nz,
     nx,
     groups,
-    q_ref,
-    k_ref,
-    v_ref,
-    og_ref,
-    in_gate_ref,
-    forget_ref,
-    extra_ref,
-    head_gain_ref,
-    tok_ref,
-    norm_gain_ref,
-    routes_ref,
-    weight_ref,
+    in_gate_hbm,
+    forget_hbm,
+    extra_hbm,
+    head_gain_hbm,
+    norm_gain_hbm,
+    routes_hbm,
+    weight_hbm,
+    tok_hbm,
+    k_hbm,
+    v_hbm,
+    q_hbm,
+    og_hbm,
     wout_hbm,
     wg_hbm,
     wu_hbm,
     wd_hbm,
     mix_ref,
     exp_ref,
+    in_gate_ref,
+    forget_ref,
+    extra_ref,
+    head_gain_ref,
+    norm_gain_ref,
+    routes_ref,
+    weight_ref,
+    tok_ref,
+    k_ref,
+    v_ref,
+    q_ref,
+    og_ref,
     wout,
     wg,
     wu,
@@ -82,18 +94,28 @@
     state_in,
     stat_out,
     stat_in,
+    own_chip,
     chip_state,
-    chip_in,
     chip_stat,
+    near_state,
+    near_stat,
+    pair_state,
+    pair_stat,
+    pairs_in,
     stats,
     scan_out,
+    top_out,
+    top_in,
     far,
     gated,
     head_part,
     parts_in,
+    partial,
     load_sem,
     pair_s,
     pair_r,
+    n_s,
+    n_r,
     z_s,
     z_r,
     x_s,
@@ -124,7 +146,7 @@
     span, dqk = q_ref.shape
     dv = v_ref.shape[1]
     tile = min(512, width)
-    hr = dqk // 2 // nz
+    hr = dqk // 2 // (nz // 2)
 
     def at(z_, c_, x_):
         return {"ep": z_ * cores + c_, "tp": x_}
@@ -145,15 +167,31 @@
             device_id_type=MESH,
         )
 
+    first_loads = [
+        pltpu.make_async_copy(src, dst, load_sem.at[4 + i])
+        for i, (src, dst) in enumerate(
+            (
+                (tok_hbm, tok_ref),
+                (routes_hbm, routes_ref),
+                (norm_gain_hbm, norm_gain_ref),
+                (in_gate_hbm, in_gate_ref),
+                (forget_hbm, forget_ref),
+                (extra_hbm, extra_ref),
+                (k_hbm, k_ref),
+                (v_hbm, v_ref),
+                (q_hbm, q_ref),
+                (og_hbm, og_ref),
+                (head_gain_hbm, head_gain_ref),
+                (weight_hbm, weight_ref),
+            )
+        )
+    ]
     loads = [
         pltpu.make_async_copy(wg_hbm.at[0], wg, load_sem.at[0]),
         pltpu.make_async_copy(wu_hbm.at[0], wu, load_sem.at[1]),
         pltpu.make_async_copy(wd_hbm.at[0], wd, load_sem.at[2]),
         pltpu.make_async_copy(wout_hbm, wout, load_sem.at[3]),
     ]
-    for load in loads:
-        load.start()
-
     barrier = pltpu.get_barrier_semaphore()
     for i in range(1, nz):
         pl.semaphore_signal(
@@ -162,6 +200,11 @@
     for i in range(1, nr):
         pl.semaphore_signal(barrier, inc=1, device_id=row_dev((r + i) % nr), device_id_type=MESH)
 
+    for load in first_loads + loads:
+        load.start()
+
+    for load in first_loads[:3]:
+        load.wait()
     t_f32 = tok_ref[...].astype(F32)
     centre = jnp.mean(t_f32, axis=1, keepdims=True)
     t_f32 = t_f32 - centre
@@ -201,31 +244,8 @@
             mm(pick, normed[:, n : n + tile]).astype(BF16).reshape(nz, blk, tile)
         )
 
-    pl.semaphore_wait(barrier, nz - 1 + nr - 1)
-
-    sends = []
-
-    def send(*args):
-        made = copy(*args)
-        made.start()
-        sends.append(made)
-        return made
-
-    def z_send(places):
-        return [
-            send(
-                out1.at[p],
-                in1.at[p],
-                z_s.at[p],
-                z_r.at[p],
-                at((z + offset(p)) % nz, c, x),
-            )
-            for p in places
-        ]
-
-    z_copies = z_send(range(min(gs, nz - 1)))
-    in1[nz - 1] = out1[nz - 1]
-
+    for load in first_loads[3:8]:
+        load.wait()
     forget = forget_ref[...]
     forget = jnp.minimum(forget, 0.0) - jnp.log1p(jnp.exp(-jnp.abs(forget))) + extra_ref[...]
     in_gate = in_gate_ref[...]
@@ -250,11 +270,37 @@
     stat_out[1:2, :] = jnp.broadcast_to(bw_top, (1, 128))
     stat_out[2:3, :] = jnp.broadcast_to(total, (1, 128))
     stat_out[3:8, :] = jnp.zeros((5, 128), F32)
+    pl.semaphore_wait(barrier, nz - 1 + nr - 1)
+
+    sends = []
+
+    def send(*args):
+        made = copy(*args)
+        made.start()
+        sends.append(made)
+        return made
+
+    def z_send(places):
+        return [
+            send(
+                out1.at[p],
+                in1.at[p],
+                z_s.at[p],
+                z_r.at[p],
+                at((z + offset(p)) % nz, c, x),
+            )
+            for p in places
+        ]
+
+
     partner = at(z, 1 - c, x)
     pair_copies = [
         send(state_out, state_in, pair_s.at[0], pair_r.at[0], partner),
         send(stat_out, stat_in, pair_s.at[1], pair_r.at[1], partner),
     ]
+
+    z_copies = z_send(range(1))
+    in1[nz - 1] = out1[nz - 1]
 
     scale = dqk**-0.5
     fw_in = jnp.where(ti >= si, through_col - through_row + in_gate, -jnp.inf)
@@ -286,20 +332,47 @@
             jnp.exp(own_log - top)[:, 0:1] * own_state[i, mine, :]
             + jnp.exp(par_log - top)[:, 0:1] * state_in[i, mine, :].astype(F32)
         )
-        chip_state[:, i * hr : (i + 1) * hr, :] = joined.astype(BF16).reshape(nz, hr, dv)
+        own_chip[i] = joined
+        chip_state[i] = joined.astype(BF16)
+    t_chip = t_own + t_par
     chip_stat[0:1, :] = f_chip
     chip_stat[1:2, :] = b_chip
-    chip_stat[2:3, :] = t_own + t_par
+    chip_stat[2:3, :] = t_chip
     chip_stat[3:8, :] = jnp.zeros((5, 128), F32)
+
+    odd = z % 2
+    later = odd == 1
+    m = z // 2
+    neighbour = at(z + 1 - 2 * odd, c, x)
+    n_pairs = nz // 2
+    next_copies = [
+        send(chip_stat, near_stat, n_s.at[0], n_r.at[0], neighbour),
+        send(chip_state.at[odd], near_state.at[c], n_s.at[1], n_r.at[1], neighbour),
+    ]
+    z_copies += z_send(range(1, min(gs, nz - 1)))
+    for made in next_copies:
+        made.wait_recv()
+    f_near, b_near, t_near = (row(near_stat, i) for i in range(3))
+    own_log = jnp.where(later, f_chip, b_chip)
+    near_log = jnp.where(later, f_near, b_near) + t_chip
+    pair_top = jnp.maximum(own_log, near_log)
+    joined = (
+        jnp.exp(own_log - pair_top)[:, 0:1] * own_chip[1 - odd]
+        + jnp.exp(near_log - pair_top)[:, 0:1] * near_state[c].astype(F32)
+    )
+    pair_state[...] = joined.astype(BF16).reshape(n_pairs, hr, dv)
+    pair_stat[0:1, :] = pair_top
+    pair_stat[1:2, :] = t_chip + t_near
+    pair_stat[2:8, :] = jnp.zeros((6, 128), F32)
     a_copies = []
-    for i in range(1, nz):
-        to = (z + i) % nz
-        dev = at(to, c, x)
-        a_copies.append(send(chip_stat, stats.at[z], t_s.at[i], t_r.at[i], dev))
-        a_copies.append(send(chip_state.at[to], chip_in.at[z], a_s.at[i], a_r.at[i], dev))
-    z_copies += z_send(range(min(gs, nz - 1), nz - 1))
-    chip_in[z] = chip_state[z]
-    stats[z] = chip_stat[...]
+    for i in range(1, n_pairs):
+        to = (m + i) % n_pairs
+        dev = at(2 * to + odd, c, x)
+        a_copies.append(send(pair_stat, stats.at[m], t_s.at[i], t_r.at[i], dev))
+        a_copies.append(send(pair_state.at[to], pairs_in.at[m], a_s.at[i], a_r.at[i], dev))
+    z_copies += z_send(range(min(gs, nz - 1), min(2 * gs, nz - 1)))
+    pairs_in[m] = pair_state[m]
+    stats[m] = pair_stat[...]
 
     ga, gb = iota((gs * blk, gs * blk), 0), iota((gs * blk, gs * blk), 1)
     lc, lg, lr = (int(math.log2(n)) for n in (cap, gs, nr))
@@ -377,32 +450,40 @@
     for made in a_copies:
         made.wait_recv()
     lanes = [pl.ds(n, 128) for n in range(0, dv, 128)]
-    tops = []
-    for i, order in ((0, range(nz)), (1, range(nz - 1, -1, -1))):
-        top = jnp.full((1, 128), lowest_log, F32)
-        my_top = top
-        memory = [jnp.zeros((hr, 128), F32) for _ in lanes]
-        for w in order:
-            my_top = jnp.where(w == z, top, my_top)
-            for lane, m in zip(lanes, memory):
-                scan_out[w, i * hr : (i + 1) * hr, lane] = m.astype(BF16)
-            state_top, state_total = stats[w, i : i + 1, :], stats[w, 2:3, :]
-            new_top = jnp.maximum(state_total + top, state_top)
-            keep = jnp.exp(state_total + top - new_top)
-            take = jnp.exp(state_top - new_top)
-            memory = [
-                keep * m + take * chip_in[w, i * hr : (i + 1) * hr, lane].astype(F32)
-                for lane, m in zip(lanes, memory)
-            ]
-            top = new_top
-        tops.append(my_top[:, 0:1])
+    top = jnp.full((1, 128), lowest_log, F32)
+    my_top = top
+    memory = [jnp.zeros((hr, 128), F32) for _ in lanes]
+    for step in range(n_pairs):
+        w = odd * step + (1 - odd) * (n_pairs - 1 - step)
+        my_top = jnp.where(w == m, top, my_top)
+        for lane, part in zip(lanes, memory):
+            scan_out[w, :, lane] = part.astype(BF16)
+        state_top, state_total = stats[w, 0:1, :], stats[w, 1:2, :]
+        new_top = jnp.maximum(state_total + top, state_top)
+        keep = jnp.exp(state_total + top - new_top)
+        take = jnp.exp(state_top - new_top)
+        memory = [
+            keep * part + take * pairs_in[w, :, lane].astype(F32)
+            for lane, part in zip(lanes, memory)
+        ]
+        top = new_top
+    top_out[...] = jnp.broadcast_to(my_top, (8, 128))
+    top_copy = send(top_out, top_in, n_s.at[2], n_r.at[2], neighbour)
+    mine_dir = 1 - odd
     b_copies = []
-    for i in range(1, nz):
-        to = (z + i) % nz
+    for i in range(1, n_pairs):
+        to = (m + i) % n_pairs
         b_copies.append(
-            send(scan_out.at[to], far.at[c, z], b_s.at[i], b_r.at[i], at(to, c, x))
-        )
-    far[c, z] = scan_out[z]
+            send(
+                scan_out.at[to],
+                far.at[mine_dir, c, m],
+                b_s.at[i],
+                b_r.at[i],
+                at(2 * to + odd, c, x),
+            )
+        )
+    far[mine_dir, c, m] = scan_out[m]
+    z_copies += z_send(range(min(2 * gs, nz - 1), nz - 1))
 
     for load in loads[:3]:
         load.wait()
@@ -411,34 +492,54 @@
             spread(g)
         if 0 <= g - 1 < groups:
             experts(g - 1)
+        if g == 1:
+            for made in b_copies:
+                made.wait_recv()
+            far_next = send(
+                far.at[mine_dir, c], far.at[mine_dir, c], n_s.at[3], n_r.at[3], neighbour
+            )
         if 0 <= g - 2 < groups:
             give_back(g - 2)
     ret_in[nz - 1] = ret_out[nz - 1]
 
-    for made in b_copies:
-        made.wait_recv()
-    far_copy = send(far.at[c], far.at[c], pair_s.at[2], pair_r.at[2], partner)
-    far_in = copy(far.at[c], far.at[1 - c], pair_s.at[2], pair_r.at[2], partner)
+    top_copy.wait_recv()
+    copy(
+        far.at[mine_dir, c], far.at[1 - mine_dir, c], n_s.at[3], n_r.at[3], neighbour
+    ).wait_recv()
+    halves = [(far.at[0], 2), (far.at[1], 3), (near_state, 4)]
+    for ref, i in halves:
+        send(ref.at[c], ref.at[c], pair_s.at[i], pair_r.at[i], partner)
+    for load in first_loads[8:]:
+        load.wait()
     scores = mm_t(q_ref[...], k_ref[...]) * scale
-    t_own, t_par, f_par, b_par = (v[:, 0:1] for v in (t_own, t_par, f_par, b_par))
+    t_par, f_par, b_par, t_near, f_near, b_near, my_top = (
+        value[:, 0:1] for value in (t_par, f_par, b_par, t_near, f_near, b_near, my_top)
+    )
+    other_top = top_in[0:1, 0:1]
     rest_col = total - before_col
-    prior_log = through_col + (tops[0] + jnp.where(first, 0.0, t_par))
-    later_log = rest_col + (tops[1] + jnp.where(first, t_par, 0.0))
+    since_start = through_col + jnp.where(first, 0.0, t_par)
+    until_end = rest_col + jnp.where(first, t_par, 0.0)
+    prior_log = since_start + jnp.where(later, t_near + my_top, other_top)
+    later_log = until_end + jnp.where(later, other_top, t_near + my_top)
+    near_log = jnp.where(later, since_start + f_near, until_end + b_near)
     pair_log = jnp.where(first, rest_col + b_par, through_col + f_par)
     row_top = jnp.maximum(
-        jnp.maximum(inner_top, prior_log), jnp.maximum(later_log, pair_log)
+        jnp.maximum(jnp.maximum(inner_top, near_log), prior_log),
+        jnp.maximum(later_log, pair_log),
     )
     weights = jnp.exp(fw_in - row_top) + jnp.exp(bw_in - row_top)
     near = (scores * weights).astype(BF16)
-    far_in.wait_recv()
+    for ref, i in halves:
+        copy(ref.at[c], ref.at[1 - c], pair_s.at[i], pair_r.at[i], partner).wait_recv()
     queries = q_ref[...]
 
     def far_memory(i):
-        return far[:, :, i * hr : (i + 1) * hr, :].reshape(dqk, dv)
+        return far[i].reshape(dqk, dv)
 
     head_rows = mm(near, v_ref[...]) + scale * (
         jnp.exp(prior_log - row_top) * mm(queries, far_memory(0))
         + jnp.exp(later_log - row_top) * mm(queries, far_memory(1))
+        + jnp.exp(near_log - row_top) * mm(queries, near_state[...].reshape(dqk, dv))
         + jnp.exp(pair_log - row_top) * mm(queries, state_in[1 - c])
     )
     head_rows = (
@@ -470,14 +571,37 @@
     share = jnp.where(places == place_col[0], to_col(weight_ref[0:1, :]), 0.0) + jnp.where(
         places == place_col[1], to_col(weight_ref[1:2, :]), 0.0
     )
-    for made in zb_copies:
+    for made in sends:
+        if all(made is not other for other in zb_copies):
+            made.wait_send()
+    early = nz - gs
+
+    def part(first_place, last_place, n):
+        returned = ret_in[first_place:last_place, :, n : n + tile]
+        return mm_split(
+            share[:, first_place * blk : last_place * blk],
+            returned.reshape((last_place - first_place) * blk, tile),
+        )
+
+    if early:
+        for made in zb_copies[:early]:
+            made.wait_recv()
+        for n in range(0, width, tile):
+            partial[:, n : n + tile] = part(0, early, n)
+    for made in zb_copies[early:]:
         made.wait_recv()
     for n in range(0, width, tile):
-        returned = ret_in[:, :, n : n + tile].reshape(nz * blk, tile)
-        exp_ref[:, n : n + tile] = mm_split(share, returned).astype(BF16)
-
-    for made in sends:
+        rest = part(early, nz, n)
+        if early:
+            rest = rest + partial[:, n : n + tile]
+        exp_ref[:, n : n + tile] = rest.astype(BF16)
+    for made in zb_copies:
         made.wait_send()
+
+
+def hand_over(mix_in, exp_in, mix_out, exp_out):
+    mix_out[...] = mix_in[...]
+    exp_out[...] = exp_in[...]
 
 
 def body(
@@ -508,7 +632,8 @@
     blk = nr * cap
     groups = 4 if nz % 4 == 0 else 1
     gs = nz // groups
-    hr = dqk // 2 // nz
+    n_pairs = nz // 2
+    hr = dqk // 2 // n_pairs
     vmem = pl.BlockSpec(memory_space=pltpu.VMEM)
     hbm = pl.BlockSpec(memory_space=pl.ANY)
     dma = pltpu.SemaphoreType.DMA
@@ -518,9 +643,21 @@
             jax.ShapeDtypeStruct((span // nx, width), BF16),
             jax.ShapeDtypeStruct((tokens, width), BF16),
         ),
-        in_specs=[vmem] * 12 + [hbm] * 4,
+        in_specs=[hbm] * 16,
         out_specs=(vmem, vmem),
         scratch_shapes=[
+            pltpu.VMEM((1, span), F32),
+            pltpu.VMEM((1, span), F32),
+            pltpu.VMEM((1, span), F32),
+            pltpu.VMEM((1, dv), F32),
+            pltpu.VMEM((1, width), F32),
+            pltpu.VMEM((2, tokens), jnp.int32),
+            pltpu.VMEM((2, tokens), F32),
+            pltpu.VMEM((tokens, width), BF16),
+            pltpu.VMEM((span, dqk), BF16),
+            pltpu.VMEM((span, dv), BF16),
+            pltpu.VMEM((span, dqk), BF16),
+            pltpu.VMEM((span, dv), BF16),
             pltpu.VMEM((dv, width), BF16),
             pltpu.VMEM((width, fe), BF16),
             pltpu.VMEM((width, fe), BF16),
@@ -540,18 +677,28 @@
             pltpu.VMEM((2, dqk, dv), BF16),
             pltpu.VMEM((8, 128), F32),
             pltpu.VMEM((8, 128), F32),
-            pltpu.VMEM((nz, 2 * hr, dv), BF16),
-            pltpu.VMEM((nz, 2 * hr, dv), BF16),
+            pltpu.VMEM((2, dqk // 2, dv), F32),
+            pltpu.VMEM((2, dqk // 2, dv), BF16),
             pltpu.VMEM((8, 128), F32),
-            pltpu.VMEM((nz, 8, 128), F32),
-            pltpu.VMEM((nz, 2 * hr, dv), BF16),
-            pltpu.VMEM((2, nz, 2 * hr, dv), BF16),
+            pltpu.VMEM((2, dqk // 2, dv), BF16),
+            pltpu.VMEM((8, 128), F32),
+            pltpu.VMEM((n_pairs, hr, dv), BF16),
+            pltpu.VMEM((8, 128), F32),
+            pltpu.VMEM((n_pairs, hr, dv), BF16),
+            pltpu.VMEM((n_pairs, 8, 128), F32),
+            pltpu.VMEM((n_pairs, hr, dv), BF16),
+            pltpu.VMEM((8, 128), F32),
+            pltpu.VMEM((8, 128), F32),
+            pltpu.VMEM((2, 2, n_pairs, hr, dv), BF16),
             pltpu.VMEM((span, dv), BF16),
             pltpu.VMEM((nx, span // nx, width), BF16),
             pltpu.VMEM((nx, span // nx, width), BF16),
+            pltpu.VMEM((tokens, width), F32),
+            dma((16,)),
+            dma((5,)),
+            dma((5,)),
             dma((4,)),
-            dma((3,)),
-            dma((3,)),
+            dma((4,)),
             dma((nz,)),
             dma((nz,)),
             dma((groups, nr)),
@@ -574,24 +721,34 @@
         ),
         name="layer_step",
     )(
-        queries,
-        head_key_rows,
-        head_value_rows,
-        output_gate_logits,
         log_input_gate,
         forget_gate_logits,
         extra_log_forget,
         head_norm_gain.reshape(1, dv),
-        expert_input_tokens,
         expert_norm_gain.reshape(1, width),
         routes.T,
         routed_expert_weight.T,
+        expert_input_tokens,
+        head_key_rows,
+        head_value_rows,
+        queries,
+        output_gate_logits,
         memory_output_matrix,
         expert_gate_matrix,
         expert_up_matrix,
         expert_down_matrix,
     )
-    return mixer_out, expert_out
+    return pl.pallas_call(
+        hand_over,
+        out_shape=(
+            jax.ShapeDtypeStruct(mixer_out.shape, BF16),
+            jax.ShapeDtypeStruct(expert_out.shape, BF16),
+        ),
+        in_specs=[vmem] * 2,
+        out_specs=(vmem,) * 2,
+        compiler_params=pltpu.CompilerParams(vmem_limit_bytes=60 * 2**20),
+        name="hand_over",
+    )(mixer_out, expert_out)
 
 
 def solution(mesh):

time: 152 us -> 144 us (0.947)
  Pallas kernels: 148 us -> 143 us
  local copies, waits for them, and re-layouts: 3.34 us -> 0 us
    pallas_call x1, Pallas kernels: 148 us -> 141 us  [body(): pl.pallas_call(functools.partial(kernel, nz, nx, groups), out_shape=(jax....]
    unnamed x2 -> x0, local copies, waits for them, and re-layouts: 3.34 us -> none
    pallas_call x0 -> x1, Pallas kernels: none -> 1.84 us  [body(): pl.pallas_call(hand_over, out_shape=(jax.ShapeDtypeStruct(mixer_out.shape...]
where the time goes in v3:
time: 144 us
  Pallas kernels  143 us (99%)
    pallas_call x1, Pallas kernels, body(): pl.pallas_call(functools.partial(kernel, nz, nx, groups), out_shape=(jax....  141 us

profile of v3, /device:TPU:33, one launch (start us, length us, event | category | flops | bytes accessed | tf_op | source)
XLA Modules:
  0.0 143.9 jit_solution(3860134292248212847)
XLA Ops:
  0.6 141.4 %layer_step.1 = (bf16[64,2048]{1,0:T(8,128)(2,1)}, bf16[64,2048]{1,0:T(8,128)(2,1)}) custom-call(f32[1,256]{1,0:T(1,128)} %in_gate_hbm.1, f32[1,256]{1,0:T(1,128)} %forget_hbm.1, f32[1,256]{1,0:T(1,128)} %extra_hbm.1, f32[1,512]{1,0:T(1,128)} %bitcast.5, f32[1,2048]{1,0:T(1,128)} %bitcast.4, s32[2,64]{1,0:T(2,128)} %bitcast.6, f32[2,64]{1,0:T(2,128)} %bitcast.7, ...), custom_call_target="tpu_custom_call" | custom-call | tf_op jit(solution)/shard_map/layer_step/pallas_call | solution.py:640
  142.0 1.8 %hand_over.1 = (bf16[64,2048]{1,0:T(8,128)(2,1)}, bf16[64,2048]{1,0:T(8,128)(2,1)}) custom-call(bf16[64,2048]{1,0:T(8,128)(2,1)} %get-tuple-element.4.mix_in, bf16[64,2048]{1,0:T(8,128)(2,1)} %get-tuple-element.5.exp_in), custom_call_target="tpu_custom_call" | custom-call | tf_op jit(solution)/shard_map/hand_over/pallas_call | solution.py:741

commit v4 on v3

--- a/solution.py
+++ b/solution.py
@@ -106,6 +106,7 @@
     scan_out,
     top_out,
     top_in,
+    passed,
     far,
     gated,
     head_part,
@@ -154,8 +155,13 @@
     def row_dev(r_):
         return at(z, r_ // nx, r_ % nx)
 
+    offsets = [half] + [(half + k) % nz for i in range(1, half) for k in (-i, i)] + [0]
+    if nz > 4:
+        offsets.remove(1)
+        offsets.insert(3, 1)
+
     def offset(p):
-        return half - (p + 1) // 2 if p % 2 else (half + p // 2) % nz if p < nz - 1 else 0
+        return offsets[p]
 
     def copy(src, dst, ssem, rsem, dev):
         return pltpu.make_async_remote_copy(
@@ -223,7 +229,7 @@
     def place(e, earlier):
         e = e.astype(jnp.int32)
         step = ((e >> int(math.log2(nr))) - z) & (nz - 1)
-        p = jnp.where(step < half, 2 * (half - step) - 1, 2 * (step - half))
+        p = sum(jnp.where(step == offset, p, 0) for p, offset in enumerate(offsets))
         return p * blk + (e & (nr - 1)) * cap + earlier.astype(jnp.int32)
 
     def one_if(mask):
@@ -467,8 +473,10 @@
             for lane, part in zip(lanes, memory)
         ]
         top = new_top
-    top_out[...] = jnp.broadcast_to(my_top, (8, 128))
-    top_copy = send(top_out, top_in, n_s.at[2], n_r.at[2], neighbour)
+    other = at((z + nz + 2 * odd - 1) % nz, c, x)
+    pass_top = jnp.maximum(my_top + pair_stat[1:2, :], pair_top)
+    top_out[...] = jnp.broadcast_to(pass_top, (8, 128))
+    top_copy = send(top_out, top_in, n_s.at[2], n_r.at[2], other)
     mine_dir = 1 - odd
     b_copies = []
     for i in range(1, n_pairs):
@@ -487,35 +495,37 @@
 
     for load in loads[:3]:
         load.wait()
-    for g in range(1, groups + 2):
-        if g < groups:
-            spread(g)
-        if 0 <= g - 1 < groups:
-            experts(g - 1)
-        if g == 1:
-            for made in b_copies:
-                made.wait_recv()
-            far_next = send(
-                far.at[mine_dir, c], far.at[mine_dir, c], n_s.at[3], n_r.at[3], neighbour
-            )
-        if 0 <= g - 2 < groups:
-            give_back(g - 2)
-    ret_in[nz - 1] = ret_out[nz - 1]
-
+    experts(0)
+    spread(1)
+    experts(1)
+    for made in b_copies:
+        made.wait_recv()
+    passed[...] = (
+        jnp.exp(my_top + pair_stat[1:2, :] - pass_top)[:, 0:1]
+        * far[mine_dir, c].reshape(dqk // 2, dv).astype(F32)
+        + jnp.exp(pair_top - pass_top)[:, 0:1]
+        * pair_state[...].reshape(dqk // 2, dv).astype(F32)
+    ).astype(BF16).reshape(n_pairs, hr, dv)
+    send(passed, far.at[mine_dir, c], n_s.at[3], n_r.at[3], other)
+    spread(2)
+    give_back(0)
+    experts(2)
+    spread(3)
+    give_back(1)
     top_copy.wait_recv()
-    copy(
-        far.at[mine_dir, c], far.at[1 - mine_dir, c], n_s.at[3], n_r.at[3], neighbour
-    ).wait_recv()
+    copy(passed, far.at[1 - mine_dir, c], n_s.at[3], n_r.at[3], other).wait_recv()
     halves = [(far.at[0], 2), (far.at[1], 3), (near_state, 4)]
     for ref, i in halves:
         send(ref.at[c], ref.at[c], pair_s.at[i], pair_r.at[i], partner)
+    experts(3)
     for load in first_loads[8:]:
         load.wait()
     scores = mm_t(q_ref[...], k_ref[...]) * scale
     t_par, f_par, b_par, t_near, f_near, b_near, my_top = (
         value[:, 0:1] for value in (t_par, f_par, b_par, t_near, f_near, b_near, my_top)
     )
-    other_top = top_in[0:1, 0:1]
+    at_end = (z == 0) | (z == nz - 1)
+    other_top = jnp.where(at_end, lowest_log, top_in[0:1, 0:1])
     rest_col = total - before_col
     since_start = through_col + jnp.where(first, 0.0, t_par)
     until_end = rest_col + jnp.where(first, t_par, 0.0)
@@ -559,6 +569,10 @@
         rs_copies.append(
             send(head_part.at[to], parts_in.at[i], rs_s.at[i], rs_r.at[i], at(z, c, to))
         )
+    give_back(2)
+    give_back(3)
+    ret_in[nz - 1] = ret_out[nz - 1]
+
     for made in rs_copies:
         made.wait_recv()
     for n in range(0, width, tile):
@@ -689,6 +703,7 @@
             pltpu.VMEM((n_pairs, hr, dv), BF16),
             pltpu.VMEM((8, 128), F32),
             pltpu.VMEM((8, 128), F32),
+            pltpu.VMEM((n_pairs, hr, dv), BF16),
             pltpu.VMEM((2, 2, n_pairs, hr, dv), BF16),
             pltpu.VMEM((span, dv), BF16),
             pltpu.VMEM((nx, span // nx, width), BF16),

time: 144 us -> 143 us (level)
  no operation moved by 1% of the time
where the time goes in v4:
time: 143 us
  Pallas kernels  142 us (99%)
    pallas_call x1, Pallas kernels, body(): pl.pallas_call(functools.partial(kernel, nz, nx, groups), out_shape=(jax....  140 us

profile of v4, /device:TPU:33, one launch (start us, length us, event | category | flops | bytes accessed | tf_op | source)
XLA Modules:
  0.0 142.7 jit_solution(11277710095148002059)
XLA Ops:
  0.6 140.2 %layer_step.1 = (bf16[64,2048]{1,0:T(8,128)(2,1)}, bf16[64,2048]{1,0:T(8,128)(2,1)}) custom-call(f32[1,256]{1,0:T(1,128)} %in_gate_hbm.1, f32[1,256]{1,0:T(1,128)} %forget_hbm.1, f32[1,256]{1,0:T(1,128)} %extra_hbm.1, f32[1,512]{1,0:T(1,128)} %bitcast.5, f32[1,2048]{1,0:T(1,128)} %bitcast.4, s32[2,64]{1,0:T(2,128)} %bitcast.6, f32[2,64]{1,0:T(2,128)} %bitcast.7, ...), custom_call_target="tpu_custom_call" | custom-call | tf_op jit(solution)/shard_map/layer_step/pallas_call | solution.py:654
  140.8 1.8 %hand_over.1 = (bf16[64,2048]{1,0:T(8,128)(2,1)}, bf16[64,2048]{1,0:T(8,128)(2,1)}) custom-call(bf16[64,2048]{1,0:T(8,128)(2,1)} %get-tuple-element.4.mix_in, bf16[64,2048]{1,0:T(8,128)(2,1)} %get-tuple-element.5.exp_in), custom_call_target="tpu_custom_call" | custom-call | tf_op jit(solution)/shard_map/hand_over/pallas_call | solution.py:756

commit v5 on v4

--- a/solution.py
+++ b/solution.py
@@ -112,6 +112,7 @@
     head_part,
     parts_in,
     partial,
+    ready,
     load_sem,
     pair_s,
     pair_r,
@@ -155,10 +156,11 @@
     def row_dev(r_):
         return at(z, r_ // nx, r_ % nx)
 
-    offsets = [half] + [(half + k) % nz for i in range(1, half) for k in (-i, i)] + [0]
-    if nz > 4:
-        offsets.remove(1)
-        offsets.insert(3, 1)
+    reach = nz // 4
+    rest = [half, 1] + [(half + k) % nz for i in range(1, half) for k in (-i, i)]
+    offsets = [reach, nz - reach]
+    offsets += [i for n, i in enumerate(rest) if i not in offsets + rest[:n]] + [0]
+    cuts = [0, 2, max(2, gs), max(2, 2 * gs), nz - 1]
 
     def offset(p):
         return offsets[p]
@@ -199,7 +201,8 @@
         pltpu.make_async_copy(wout_hbm, wout, load_sem.at[3]),
     ]
     barrier = pltpu.get_barrier_semaphore()
-    for i in range(1, nz):
+    close = [i for i in range(1, nz) if min(i, nz - i) <= reach]
+    for i in close:
         pl.semaphore_signal(
             barrier, inc=1, device_id=at((z + i) % nz, c, x), device_id_type=MESH
         )
@@ -276,7 +279,9 @@
     stat_out[1:2, :] = jnp.broadcast_to(bw_top, (1, 128))
     stat_out[2:3, :] = jnp.broadcast_to(total, (1, 128))
     stat_out[3:8, :] = jnp.zeros((5, 128), F32)
-    pl.semaphore_wait(barrier, nz - 1 + nr - 1)
+    pl.semaphore_wait(barrier, len(close) + nr - 1)
+    for to in (z + reach, z + nz - reach):
+        pl.semaphore_signal(ready, inc=1, device_id=at(to % nz, c, x), device_id_type=MESH)
 
     sends = []
 
@@ -305,7 +310,7 @@
         send(stat_out, stat_in, pair_s.at[1], pair_r.at[1], partner),
     ]
 
-    z_copies = z_send(range(1))
+    z_copies = z_send(range(cuts[0], cuts[1]))
     in1[nz - 1] = out1[nz - 1]
 
     scale = dqk**-0.5
@@ -355,7 +360,8 @@
         send(chip_stat, near_stat, n_s.at[0], n_r.at[0], neighbour),
         send(chip_state.at[odd], near_state.at[c], n_s.at[1], n_r.at[1], neighbour),
     ]
-    z_copies += z_send(range(1, min(gs, nz - 1)))
+    pl.semaphore_wait(ready, 2)
+    z_copies += z_send(range(cuts[1], cuts[2]))
     for made in next_copies:
         made.wait_recv()
     f_near, b_near, t_near = (row(near_stat, i) for i in range(3))
@@ -376,7 +382,7 @@
         dev = at(2 * to + odd, c, x)
         a_copies.append(send(pair_stat, stats.at[m], t_s.at[i], t_r.at[i], dev))
         a_copies.append(send(pair_state.at[to], pairs_in.at[m], a_s.at[i], a_r.at[i], dev))
-    z_copies += z_send(range(min(gs, nz - 1), min(2 * gs, nz - 1)))
+    z_copies += z_send(range(cuts[2], cuts[3]))
     pairs_in[m] = pair_state[m]
     stats[m] = pair_stat[...]
 
@@ -491,7 +497,7 @@
             )
         )
     far[mine_dir, c, m] = scan_out[m]
-    z_copies += z_send(range(min(2 * gs, nz - 1), nz - 1))
+    z_copies += z_send(range(cuts[3], cuts[4]))
 
     for load in loads[:3]:
         load.wait()
@@ -709,6 +715,7 @@
             pltpu.VMEM((nx, span // nx, width), BF16),
             pltpu.VMEM((nx, span // nx, width), BF16),
             pltpu.VMEM((tokens, width), F32),
+            pltpu.SemaphoreType.REGULAR,
             dma((16,)),
             dma((5,)),
             dma((5,)),

time: 143 us -> 141 us (0.986)
    pallas_call x1, Pallas kernels: 140 us -> 139 us  [body(): pl.pallas_call(functools.partial(kernel, nz, nx, groups), out_shape=(jax....]
where the time goes in v5:
time: 141 us
  Pallas kernels  141 us (100%)
    pallas_call x1, Pallas kernels, body(): pl.pallas_call(functools.partial(kernel, nz, nx, groups), out_shape=(jax....  139 us

profile of v5, /device:TPU:33, one launch (start us, length us, event | category | flops | bytes accessed | tf_op | source)
XLA Modules:
  0.0 141.2 jit_solution(6949689059285981507)
XLA Ops:
  0.6 138.7 %layer_step.1 = (bf16[64,2048]{1,0:T(8,128)(2,1)}, bf16[64,2048]{1,0:T(8,128)(2,1)}) custom-call(f32[1,256]{1,0:T(1,128)} %in_gate_hbm.1, f32[1,256]{1,0:T(1,128)} %forget_hbm.1, f32[1,256]{1,0:T(1,128)} %extra_hbm.1, f32[1,512]{1,0:T(1,128)} %bitcast.5, f32[1,2048]{1,0:T(1,128)} %bitcast.4, s32[2,64]{1,0:T(2,128)} %bitcast.6, f32[2,64]{1,0:T(2,128)} %bitcast.7, ...), custom_call_target="tpu_custom_call" | custom-call | tf_op jit(solution)/shard_map/layer_step/pallas_call | solution.py:660
  139.4 1.8 %hand_over.1 = (bf16[64,2048]{1,0:T(8,128)(2,1)}, bf16[64,2048]{1,0:T(8,128)(2,1)}) custom-call(bf16[64,2048]{1,0:T(8,128)(2,1)} %get-tuple-element.4.mix_in, bf16[64,2048]{1,0:T(8,128)(2,1)} %get-tuple-element.5.exp_in), custom_call_target="tpu_custom_call" | custom-call | tf_op jit(solution)/shard_map/hand_over/pallas_call | solution.py:763

commit v6 on v5

--- a/solution.py
+++ b/solution.py
@@ -61,6 +61,8 @@
     wg_hbm,
     wu_hbm,
     wd_hbm,
+    mix_hbm,
+    exp_hbm,
     mix_ref,
     exp_ref,
     in_gate_ref,
@@ -113,6 +115,7 @@
     parts_in,
     partial,
     ready,
+    store_sem,
     load_sem,
     pair_s,
     pair_r,
@@ -586,6 +589,8 @@
         for i in range(1, nx):
             mixed = mixed + parts_in[i, :, n : n + tile].astype(F32)
         mix_ref[:, n : n + tile] = mixed.astype(BF16)
+    stores = [pltpu.make_async_copy(mix_ref, mix_hbm, store_sem.at[0])]
+    stores[0].start()
 
     places = iota((tokens, nz * blk), 1)
     share = jnp.where(places == place_col[0], to_col(weight_ref[0:1, :]), 0.0) + jnp.where(
@@ -615,13 +620,41 @@
         if early:
             rest = rest + partial[:, n : n + tile]
         exp_ref[:, n : n + tile] = rest.astype(BF16)
+        stores.append(
+            pltpu.make_async_copy(
+                exp_ref.at[:, n : n + tile],
+                exp_hbm.at[:, n : n + tile],
+                store_sem.at[len(stores)],
+            )
+        )
+        stores[-1].start()
     for made in zb_copies:
         made.wait_send()
-
-
-def hand_over(mix_in, exp_in, mix_out, exp_out):
-    mix_out[...] = mix_in[...]
-    exp_out[...] = exp_in[...]
+    for made in stores:
+        made.wait()
+
+
+def hand_over(mix_in, exp_in, mix_out, exp_out, mix_ref, exp_ref, in_sem, out_sem):
+    ways = ((mix_in, mix_ref, mix_out), (exp_in, exp_ref, exp_out))
+    moves = []
+    for i, (src, held, dst) in enumerate(ways):
+        half = src.shape[0] // 2
+        for k in range(2):
+            part = pl.ds(k * half, half)
+            n = 2 * i + k
+            moves.append(
+                (
+                    pltpu.make_async_copy(src.at[part], held.at[part], in_sem.at[n]),
+                    pltpu.make_async_copy(held.at[part], dst.at[part], out_sem.at[n]),
+                )
+            )
+    for come, _ in moves:
+        come.start()
+    for come, leave in moves:
+        come.wait()
+        leave.start()
+    for _, leave in moves:
+        leave.wait()
 
 
 def body(
@@ -664,8 +697,10 @@
             jax.ShapeDtypeStruct((tokens, width), BF16),
         ),
         in_specs=[hbm] * 16,
-        out_specs=(vmem, vmem),
+        out_specs=(hbm, hbm),
         scratch_shapes=[
+            pltpu.VMEM((span // nx, width), BF16),
+            pltpu.VMEM((tokens, width), BF16),
             pltpu.VMEM((1, span), F32),
             pltpu.VMEM((1, span), F32),
             pltpu.VMEM((1, span), F32),
@@ -716,6 +751,7 @@
             pltpu.VMEM((nx, span // nx, width), BF16),
             pltpu.VMEM((tokens, width), F32),
             pltpu.SemaphoreType.REGULAR,
+            dma((1 + width // min(512, width),)),
             dma((16,)),
             dma((5,)),
             dma((5,)),
@@ -766,8 +802,14 @@
             jax.ShapeDtypeStruct(mixer_out.shape, BF16),
             jax.ShapeDtypeStruct(expert_out.shape, BF16),
         ),
-        in_specs=[vmem] * 2,
-        out_specs=(vmem,) * 2,
+        in_specs=[hbm] * 2,
+        out_specs=(hbm,) * 2,
+        scratch_shapes=[
+            pltpu.VMEM(mixer_out.shape, BF16),
+            pltpu.VMEM(expert_out.shape, BF16),
+            dma((4,)),
+            dma((4,)),
+        ],
         compiler_params=pltpu.CompilerParams(vmem_limit_bytes=60 * 2**20),
         name="hand_over",
     )(mixer_out, expert_out)

time: 141 us -> 141 us (level)
  no operation moved by 1% of the time
where the time goes in v6:
time: 141 us
  Pallas kernels  140 us (99%)
    pallas_call x1, Pallas kernels, body(): pl.pallas_call(functools.partial(kernel, nz, nx, groups), out_shape=(jax....  139 us

profile of v6, /device:TPU:33, one launch (start us, length us, event | category | flops | bytes accessed | tf_op | source)
XLA Modules:
  0.0 141.0 jit_solution(8830650054708788170)
XLA Ops:
  0.6 138.5 %layer_step.1 = (bf16[64,2048]{1,0:T(8,128)(2,1)}, bf16[64,2048]{1,0:T(8,128)(2,1)}) custom-call(f32[1,256]{1,0:T(1,128)} %in_gate_hbm.1, f32[1,256]{1,0:T(1,128)} %forget_hbm.1, f32[1,256]{1,0:T(1,128)} %extra_hbm.1, f32[1,512]{1,0:T(1,128)} %bitcast.5, f32[1,2048]{1,0:T(1,128)} %bitcast.4, s32[2,64]{1,0:T(2,128)} %bitcast.6, f32[2,64]{1,0:T(2,128)} %bitcast.7, ...), custom_call_target="tpu_custom_call" | custom-call | tf_op jit(solution)/shard_map/layer_step/pallas_call | solution.py:693
  139.2 1.8 %hand_over.1 = (bf16[64,2048]{1,0:T(8,128)(2,1)}, bf16[64,2048]{1,0:T(8,128)(2,1)}) custom-call(bf16[64,2048]{1,0:T(8,128)(2,1)} %get-tuple-element.4.mix_in, bf16[64,2048]{1,0:T(8,128)(2,1)} %get-tuple-element.5.exp_in), custom_call_target="tpu_custom_call" | custom-call | tf_op jit(solution)/shard_map/hand_over/pallas_call | solution.py:799
